TPU v7x, 256 devices: a whole 4x4x8 slice. The times are simulated.
256 devices in a mesh: sp: 32 (over z, y), tp: 8 (over x, core).
Axes of the slice: x: 4, y: 4, z: 8, core: 2. Of those that a mesh axis runs over, the one named last changes fastest.
Arguments:
- query_a: bfloat16 [6144, 2048], P('sp', 'tp'), may hold values from -7.5 to 7.5
- key_a: bfloat16 [6144, 1024], P('sp', 'tp'), may hold values from -7.5 to 7.5
- value_a: bfloat16 [6144, 1024], P('sp', 'tp'), may hold values from -6 to 6
- query_b: bfloat16 [6144, 2048], P('sp', 'tp'), may hold values from -7.5 to 7.5
- key_b: bfloat16 [6144, 512], P('sp', 'tp'), may hold values from -7.5 to 7.5
- value_b: bfloat16 [6144, 512], P('sp', 'tp'), may hold values from -6 to 6
- gain_a: float32 [2, 128], replicated, may hold values from 1 to 6.5
- gain_b: float32 [2, 64], replicated, may hold values from 1 to 8.5
- out_a: bfloat16 [2048, 4096], P('tp'), may hold values from -0.5 to 0.5
- out_b: bfloat16 [2048, 4096], P('tp'), may hold values from -0.5 to 0.5
- residual: bfloat16 [6144, 4096], P('sp'), may hold values from -6 to 6
- norm_gain: float32 [4096], replicated, may hold values from 0.1 to 1.9
- gate_weight: bfloat16 [4096, 6144], P('sp', 'tp'), may hold values from -0.09375 to 0.09375
- up_weight: bfloat16 [4096, 6144], P('sp', 'tp'), may hold values from -0.09375 to 0.09375
- down_weight: bfloat16 [6144, 4096], P('tp', 'sp'), may hold values from -0.3125 to 0.3125
Outputs:
- output: bfloat16 [6144, 4096], P(('sp', 'tp'))
All inputs are finite; a program needn't handle non-finite values.
Results may differ from a plain program's by a relative error of at most 0.017.
The roundings to bfloat16 on the way count: a program that leaves them out, or rounds other values in their place, can miss the bound.
Values may be sent and summed in bfloat16 or wider, within the bound.
A program may use at most 128 MiB of HBM per device.

v0:
```python
import jax
import jax.numpy as jnp
from jax import lax
from jax.sharding import PartitionSpec as P

HEAD_A = 128
HEAD_B = 64
GRID_W = 64


epsilon = 1e-06
theta_base = 10000.0


def rows_first(arrays, axis, dims):
    turned = [jnp.moveaxis(a, dim, 0) for a, dim in zip(arrays, dims)]
    both = jnp.concatenate([t.reshape(len(t), -1) for t in turned], axis=1)
    filled, at, outs = (lax.all_gather(both, axis, axis=0, tiled=True), 0, [])
    for t, dim in zip(turned, dims):
        share = filled[:, at : at + t[0].size].reshape(-1, *t.shape[1:])
        outs.append(jnp.moveaxis(share, 0, dim))
        at += t[0].size
    return tuple(outs)


def side_by_side(arrays, axis, dim, along):
    widths = [a.shape[along] for a in arrays]
    both = jnp.concatenate(arrays, axis=along)
    filled = lax.all_gather(both, axis, axis=dim, tiled=True)
    return tuple(jnp.split(filled, [sum(widths[:k]) for k in range(1, len(widths))], axis=along))


def cut_along(value, dim, devices):
    dims = value.shape
    parts = value.reshape(*dims[:dim], devices, dims[dim] // devices, *dims[dim + 1 :])
    return jnp.moveaxis(parts, dim, 0)


def sum_at_owner(value, axis, dim):
    parts = cut_along(value, dim, lax.axis_size(axis))
    arrived = lax.all_to_all(parts, axis, split_axis=0, concat_axis=0, tiled=True)
    return arrived.astype(jnp.float32).sum(axis=0)


def copy_for_each(value, axis):
    devices = lax.axis_size(axis)
    return lax.all_to_all(
        jnp.broadcast_to(value[None], (devices, *value.shape)), axis, 0, 0, tiled=True
    )


def laid_out(parts, dim):
    dims = list(parts.shape[1:])
    dims[dim] *= parts.shape[0]
    return jnp.moveaxis(parts, 0, dim).reshape(dims)


def gathered_copies(value, axis, dim):
    parts = copy_for_each(value, axis)
    return laid_out(parts, dim)


def rotate(inputs, num_heads, head_size, first_pos, gain):
    tok_rows = inputs.shape[0]
    vectors = inputs.astype(jnp.float32).reshape(tok_rows, num_heads, head_size)
    vectors = (
        vectors * lax.rsqrt(jnp.mean(vectors * vectors, axis=-1, keepdims=True) + epsilon) * gain
    )
    position = first_pos + jnp.arange(tok_rows, dtype=jnp.int32)
    grid_row = (position // GRID_W).astype(jnp.float32)
    grid_col = (position % GRID_W).astype(jnp.float32)
    quarter = head_size // 4
    inv_freq = theta_base ** (-4.0 * jnp.arange(quarter, dtype=jnp.float32) / head_size)
    angle_row = grid_row[:, None] * inv_freq[None, :]
    angle_col = grid_col[:, None] * inv_freq[None, :]
    angles = jnp.concatenate([angle_row, angle_row, angle_col, angle_col], axis=-1)
    quarters = vectors.reshape(tok_rows, num_heads, 4, quarter)
    rotated = jnp.stack(
        [-quarters[:, :, 1], quarters[:, :, 0], -quarters[:, :, 3], quarters[:, :, 2]], axis=2
    )
    rotated = rotated.reshape(tok_rows, num_heads, head_size)
    result = vectors * jnp.cos(angles)[:, None, :] + rotated * jnp.sin(angles)[:, None, :]
    return result.reshape(tok_rows, num_heads * head_size).astype(jnp.bfloat16)


def start_state(kv_heads, groups, tok_rows, head_size):
    return (
        jnp.full((kv_heads, groups, tok_rows), -1e30, jnp.float32),
        jnp.zeros((kv_heads, groups, tok_rows), jnp.float32),
        jnp.zeros((kv_heads, groups, tok_rows, head_size), jnp.float32),
    )


def attend(state, queries, key_rows, values, head_size):
    run_max, run_sum, run_acc = state
    kv_heads = key_rows.shape[1] // head_size
    groups = run_max.shape[1]
    q_heads = queries.reshape(queries.shape[0], kv_heads, groups, head_size)
    k_heads = key_rows.reshape(key_rows.shape[0], kv_heads, head_size)
    v_heads = values.reshape(values.shape[0], kv_heads, head_size)
    scores = jnp.einsum(
        "tkgd,pkd->kgtp", q_heads, k_heads, preferred_element_type=jnp.float32
    ) * head_size ** (-0.5)
    new_max = jnp.maximum(run_max, jnp.max(scores, axis=-1))
    exp_scores = jnp.exp(scores - new_max[..., None])
    new_sum = jnp.sum(exp_scores, axis=-1)
    new_acc = jnp.einsum(
        "kgtp,pkd->kgtd",
        exp_scores.astype(jnp.bfloat16),
        v_heads,
        preferred_element_type=jnp.float32,
    )
    return (new_max, new_sum, new_acc)


def finish(state, num_cols):
    blended = state[2] / state[1][..., None]
    return blended.transpose(2, 0, 1, 3).reshape(blended.shape[2], num_cols).astype(jnp.bfloat16)


def normalize(mixed_rows, gain):
    scale = lax.rsqrt(jnp.mean(mixed_rows * mixed_rows, axis=-1, keepdims=True) + epsilon)
    return (mixed_rows * scale * gain).astype(jnp.bfloat16)


def on_device(
    query_a,
    key_a,
    value_a,
    query_b,
    key_b,
    value_b,
    gain_a,
    gain_b,
    out_a,
    out_b,
    residual,
    norm_gain,
    gate_weight,
    up_weight,
    down_weight,
):
    tok_rows = query_a.shape[0]
    first_pos = lax.axis_index("sp") * tok_rows
    heads_a = query_a.shape[1] // HEAD_A
    heads_b = query_b.shape[1] // HEAD_B
    kv_heads_a = key_a.shape[1] // HEAD_A
    kv_heads_b = key_b.shape[1] // HEAD_B
    kv_width_b = kv_heads_b * HEAD_B
    turned_qa = rotate(query_a, heads_a, HEAD_A, first_pos, gain_a[0])
    turned_ka = rotate(key_a, kv_heads_a, HEAD_A, first_pos, gain_a[1])
    turned_qb = rotate(query_b, heads_b, HEAD_B, first_pos, gain_b[0])
    turned_kb = rotate(key_b, kv_heads_b, HEAD_B, first_pos, gain_b[1])
    pair_b = jnp.concatenate([turned_kb, value_b], axis=1)
    gate_full, up_full, down_full = rows_first(
        (gate_weight, up_weight, down_weight), "sp", (0, 0, 1)
    )
    initial = (
        start_state(kv_heads_a, heads_a // kv_heads_a, tok_rows, HEAD_A),
        start_state(kv_heads_b, heads_b // kv_heads_b, tok_rows, HEAD_B),
    )
    pieces = side_by_side((turned_ka, value_a, pair_b), "sp", 0, 1)
    state_a = attend(initial[0], turned_qa, pieces[0], pieces[1], HEAD_A)
    state_b = attend(
        initial[1], turned_qb, pieces[2][:, :kv_width_b], pieces[2][:, kv_width_b:], HEAD_B
    )
    attn_a = finish(state_a, query_a.shape[1])
    attn_b = finish(state_b, query_b.shape[1])
    own_rows = tok_rows // lax.axis_size("tp")
    own_start = lax.axis_index("tp") * own_rows
    head_sum = sum_at_owner(
        (
            jnp.dot(attn_a, out_a, preferred_element_type=jnp.float32)
            + jnp.dot(attn_b, out_b, preferred_element_type=jnp.float32)
        ).astype(jnp.bfloat16),
        "tp",
        0,
    )
    own_resid = lax.dynamic_slice_in_dim(residual, own_start, own_rows, 0)
    mixed_rows = own_resid.astype(jnp.float32) + head_sum
    normed = gathered_copies(normalize(mixed_rows, norm_gain), "tp", 0)
    gate_act = jnp.dot(normed, gate_full, preferred_element_type=jnp.float32)
    up_act = jnp.dot(normed, up_full, preferred_element_type=jnp.float32)
    hidden = (jax.nn.silu(gate_act) * up_act).astype(jnp.bfloat16)
    branch_sum = sum_at_owner(
        jnp.dot(hidden, down_full, preferred_element_type=jnp.float32).astype(jnp.bfloat16), "tp", 0
    )
    return (mixed_rows + 0.5 * branch_sum).astype(jnp.bfloat16)


def solution(mesh):
    return jax.shard_map(
        on_device,
        mesh=mesh,
        in_specs=(
            P("sp", "tp"),
            P("sp", "tp"),
            P("sp", "tp"),
            P("sp", "tp"),
            P("sp", "tp"),
            P("sp", "tp"),
            P(),
            P(),
            P("tp", None),
            P("tp", None),
            P("sp", None),
            P(),
            P("sp", "tp"),
            P("sp", "tp"),
            P("tp", "sp"),
        ),
        out_specs=P(("sp", "tp"), None),
        check_vma=False,
    )
```

profile of v0, /device:TPU:1, one launch (start us, length us, event | category | flops | bytes accessed | tf_op | source)
XLA Modules:
  0.0 315.2 jit_solution(1627057619854827771)
XLA Ops:
  6.6 0.9 slice_bitcast_fusion.20
  7.4 0.8 fusion.64
  8.2 0.8 fusion.65
  9.1 0.8 slice_bitcast_fusion.21
  9.9 0.9 fusion.59
  10.8 0.9 fusion.60
  11.7 0.1 copy.42
  11.8 0.1 copy.43
  12.0 0.1 broadcast_multiply_fusion.1
  12.2 0.9 fusion.69
  13.1 0.1 copy.44
  13.2 0.9 copy.45
  14.1 1.3 add_convert_fusion.1
  15.3 1.6 pad_maximum_fusion.3
  17.0 1.1 copy.54
  18.0 1.1 copy.55
  19.1 1.8 pad_maximum_fusion
  20.9 0.1 copy.51
  21.2 0.1 copy.47
  21.3 0.1 copy.48
  21.4 0.1 copy.46
  21.8 0.1 fusion.54
  22.0 0.1 multiply_multiply_fusion.1
  22.2 0.1 fusion.57
  22.3 77.9 %all-gather.3.cloned.1.call-done = bf16[6144,384]{1,0:T(8,128)(2,1)} async-done(((bf16[192,384]{1,0:T(8,128)(2,1)}), bf16[6144,384]{1,0:T(8,128)(2,1)}) %all-gather.3.cloned.1.call-update) | async-done | bytes 4718608 | tf_op jit(solution)/shard_map/all_gather | solution.py:29
  100.2 2.9 bitcast_reduce_fusion.1
  103.1 1.4 fusion.7
  104.6 0.9 copy-done.3
  105.5 1.4 fusion.38
  106.9 0.1 copy.50
  107.0 8.0 %bitcast_reduce_fusion = (f32[4,192]{1,0:T(4,128)S(1)}, f32[6144,192,4]{0,1,2:T(8,128)}) fusion(bf16[192,4,64]{0,2,1:T(8,128)(2,1)S(1)} %bitcast.178, bf16[6144,384]{1,0:T(8,128)(2,1)S(1)} %copy-done.3), kind=kOutput, calls=%fused_computation.1 | convolution fusion | flops 613416192 | bytes 20581376 | tf_op jit(solution)/shard_map/tkgd,pkd->kgtp/dot_general | solution.py:101
  115.1 2.2 fusion.61
  117.3 9.7 %fusion.1 = f32[4,192]{1,0:T(4,128)S(1)} fusion(f32[6144,192,4]{0,1,2:T(8,128)} %get-tuple-element.40, f32[4,192]{1,0:T(4,128)S(1)} %broadcast_maximum_fusion), kind=kLoop, calls=%fused_computation.3 | loop fusion | flops 14155008 | bytes 18880512 | tf_op jit(solution)/shard_map/reduce_sum | solution.py:106
  127.0 10.7 %fusion.44 = bf16[4,192,64]{1,2,0:T(8,128)(2,1)S(1)} fusion(bf16[6144,384]{1,0:T(8,128)(2,1)} %all-gather.3.cloned.1.call-done, f32[6144,192,4]{0,1,2:T(8,128)} %get-tuple-element.40, f32[4,192]{1,0:T(4,128)S(1)} %broadcast_maximum_fusion, f32[4,192]{1,0:T(4,128)S(1)} %fusion.1), kind=kOutput, calls=%fused_computation.38 | convolution fusion | flops 618233856 | bytes 20551680 | tf_op jit(solution)/shard_map/kgtp,pkd->kgtd/dot_general | solution.py:107
  137.7 1.8 fusion.15
  139.5 9.0 %all-to-all-start = ((bf16[8,24,4096]{2,1,0:T(8,128)(2,1)}), bf16[8,24,4096]{2,1,0:T(8,128)(2,1)S(1)}, u32[]{:S(2)}, u32[]{:S(2)}) async-start(bf16[8,24,4096]{2,1,0:T(8,128)(2,1)} %bitcast.171), calls=%async_computation | async-start | bytes 3145728 | tf_op jit(solution)/shard_map/all_to_all | solution.py:41
  148.5 20.6 %all-to-all-done = bf16[8,24,4096]{2,1,0:T(8,128)(2,1)S(1)} async-done(((bf16[8,24,4096]{2,1,0:T(8,128)(2,1)}), bf16[8,24,4096]{2,1,0:T(8,128)(2,1)S(1)}, u32[]{:S(2)}, u32[]{:S(2)}) %all-to-all-start) | async-done | bytes 1572896 | tf_op jit(solution)/shard_map/all_to_all | solution.py:41
  169.1 0.2 convert_reduce_fusion.1
  169.3 1.1 multiply_reduce_fusion
  170.4 1.1 multiply_convert_fusion
  171.5 0.2 broadcast_in_dim.8
  171.7 24.7 %all_to_all.15 = bf16[8,24,4096]{2,1,0:T(8,128)(2,1)} all-to-all(bf16[8,24,4096]{2,1,0:T(8,128)(2,1)S(1)} %broadcast_in_dim.8), channel_id=1, replica_groups=mesh['sp'=32,'tp'=8] {'tp'}, dimensions={0} | all-to-all | bytes 3145728 | tf_op jit(solution)/shard_map/all_to_all | solution.py:47
  196.3 65.0 %all-gather.5.cloned.1.call-done = bf16[4096,2304]{0,1:T(8,128)(2,1)} async-done(((bf16[128,2304]{0,1:T(8,128)(2,1)}), bf16[4096,2304]{0,1:T(8,128)(2,1)}) %all-gather.5.cloned.1.call-update) | async-done | bytes 18874384 | tf_op jit(solution)/shard_map/all_gather | solution.py:18
  261.3 5.5 %fusion.13 = f32[192,768]{1,0:T(8,128)S(1)} fusion(bf16[192,4096]{1,0:T(8,128)(2,1)} %bitcast.174, bf16[4096,2304]{0,1:T(8,128)(2,1)} %all-gather.5.cloned.1.call-done), kind=kOutput, calls=%fused_computation.17 | convolution fusion | flops 1207959552 | bytes 8454144 | tf_op jit(solution)/shard_map/dot_general | solution.py:182
  266.8 10.9 %fusion.16 = bf16[192,4096]{1,0:T(8,128)(2,1)} fusion(bf16[4096,2304]{0,1:T(8,128)(2,1)} %all-gather.5.cloned.1.call-done, bf16[192,4096]{1,0:T(8,128)(2,1)} %bitcast.175, f32[192,768]{1,0:T(8,128)S(1)} %fusion.13), kind=kOutput, calls=%fused_computation.21 | convolution fusion | flops 2417590272 | bytes 16318464 | tf_op jit(solution)/shard_map/dot_general | solution.py:186
  277.7 28.8 %all_to_all.16 = bf16[8,24,4096]{2,1,0:T(8,128)(2,1)S(1)} all-to-all(bf16[8,24,4096]{2,1,0:T(8,128)(2,1)} %bitcast.176), channel_id=1, replica_groups=mesh['sp'=32,'tp'=8] {'tp'}, dimensions={0} | all-to-all | bytes 3145728 | tf_op jit(solution)/shard_map/all_to_all | solution.py:41
  306.5 0.2 convert_reduce_fusion
  306.7 1.7 add_convert_fusion
  (46 shorter events, 0.8 us)
Async XLA Ops:
  6.5 108.5 %copy-start = (bf16[256,4096]{1,0:T(8,128)(2,1)S(1)}, bf16[256,4096]{1,0:T(8,128)(2,1)}, u32[]{:S(2)}) copy-start(bf16[256,4096]{1,0:T(8,128)(2,1)} %param.23) | copy-start | bytes 6291460
  6.5 14.4 %copy-start.5 = (bf16[192,256]{1,0:T(8,128)(2,1)S(1)}, bf16[192,256]{1,0:T(8,128)(2,1)}, u32[]{:S(2)}) copy-start(bf16[192,256]{1,0:T(8,128)(2,1)} %param.18) | copy-start | bytes 294916
  6.5 14.9 %copy-start.6 = (bf16[192,256]{1,0:T(8,128)(2,1)S(1)}, bf16[192,256]{1,0:T(8,128)(2,1)}, u32[]{:S(2)}) copy-start(bf16[192,256]{1,0:T(8,128)(2,1)} %param.15) | copy-start | bytes 294916
  6.5 93.6 %all-gather.3.cloned.1.call-start = ((), (), s32[]{:S(2)}) async-start(), calls=%async_computation.3 | async-start | bytes 4866048 | tf_op jit(solution)/shard_map/all_gather | solution.py:29
  16.9 244.4 %all-gather.5.cloned.1.call-start = ((), (), s32[]{:S(2)}) async-start(), calls=%async_computation.4 | async-start | bytes 19464192 | tf_op jit(solution)/shard_map/all_gather | solution.py:18
  103.1 2.3 copy-start.3
  127.0 10.7 %copy-start.2 = (f32[192,4096]{1,0:T(8,128)S(1)}, f32[192,4096]{1,0:T(8,128)}, u32[]{:S(2)}) copy-start(f32[192,4096]{1,0:T(8,128)} %fusion.61) | copy-start | bytes 9437188
  127.0 10.7 %copy-start.4 = (bf16[256,4096]{1,0:T(8,128)(2,1)S(1)}, bf16[256,4096]{1,0:T(8,128)(2,1)}, u32[]{:S(2)}) copy-start(bf16[256,4096]{1,0:T(8,128)(2,1)} %param.24) | copy-start | bytes 6291460
  137.7 32.7 %copy-start.7 = (f32[4096]{0:T(1024)S(1)}, f32[4096]{0:T(1024)}, u32[]{:S(2)}) copy-start(f32[4096]{0:T(1024)} %param.26) | copy-start | bytes 49156
  139.5 29.6 %all-to-all-start = ((bf16[8,24,4096]{2,1,0:T(8,128)(2,1)}), bf16[8,24,4096]{2,1,0:T(8,128)(2,1)S(1)}, u32[]{:S(2)}, u32[]{:S(2)}) async-start(bf16[8,24,4096]{2,1,0:T(8,128)(2,1)} %bitcast.171), calls=%async_computation | async-start | bytes 3145728 | tf_op jit(solution)/shard_map/all_to_all | solution.py:41
  266.8 41.6 %copy-start.1 = (bf16[256,4096]{1,0:T(8,128)(2,1)S(1)}, bf16[256,4096]{1,0:T(8,128)(2,1)}, u32[]{:S(2)}) copy-start(bf16[256,4096]{1,0:T(8,128)(2,1)} %param.23) | copy-start | bytes 6291460
Sparse Core Ops, SparseCore 0:
  17.0 83.1 all-gather.2
  102.6 158.6 all-gather.4
where the time goes:
time: 316 us; the launch traced here: 315 us
  waiting for transfers between devices  163 us (52%)
  blocking collectives  53.4 us (17%)
  matrix products  43.4 us (14%)
  other arithmetic  25.2 us (8%)
  between operations  13.8 us (4%)
  starting transfers between devices  9.09 us (3%)
  local copies, waits for them, and re-layouts  6.82 us (2%)
    all_gather x1, waiting for transfers between devices, side_by_side(): filled = lax.all_gather(both, axis, axis=dim, tiled=True)  77.9 us
    all_gather x1, waiting for transfers between devices, rows_first(): filled, at, outs = (lax.all_gather(both, axis, axis=0, tiled=True), 0, [])  65 us
    all_to_all x1, blocking collectives, sum_at_owner(): lax.all_to_all(parts, axis, split_axis=0, concat_axis=0, tiled=True)  28.8 us
    all_to_all x1, blocking collectives, copy_for_each(): lax.all_to_all(jnp.broadcast_to(value[None], (devices, *value.shape)), ax...  24.7 us
    all_to_all x1, waiting for transfers between devices, sum_at_owner(): lax.all_to_all(parts, axis, split_axis=0, concat_axis=0, tiled=True)  20.6 us
    dot_general x2, matrix products, attend(): jnp.einsum('kgtp,pkd->kgtd', exp_scores.astype(jnp.bfloat16), v_heads, pr...  12.1 us
    reduce_sum x2, other arithmetic, attend(): new_sum = jnp.sum(exp_scores, axis=-1)  11.1 us
    dot_general x2, matrix products, attend(): jnp.einsum('tkgd,pkd->kgtp', q_heads, k_heads, preferred_element_type=jnp...  11 us
  transfers between devices with their start and end apart: 3, of which 3 were waited for; matrix products, arithmetic and copies ran while one was open for 15% of the time, Pallas kernels for 0%

commit v1 on v0

v1 whole, which is shorter than its diff:
```python
import jax
import jax.numpy as jnp
import numpy as np
from jax import lax
from jax.experimental import pallas as pl
from jax.experimental.pallas import tpu as pltpu
from jax.sharding import PartitionSpec as P

NZ, NY, NX, NC = 8, 4, 4, 2
ROWS = 192
OWN = 24
HEAD_A, HEAD_B, GRID_W = 128, 64, 64
D = 4096
HID = 384
EPS = 1e-06
BASE = 10000.0
MESH = pl.DeviceIdType.MESH
F32, BF16 = jnp.float32, jnp.bfloat16


def turn_tables():
    rows, cols = [], []
    for head in (HEAD_A, HEAD_B):
        quarter = head // 4
        freq = np.float32(BASE) ** (-4.0 * np.arange(quarter, dtype=np.float32) / head).astype(np.float32)
        lane = np.arange(128)
        lane_freq = freq[lane % quarter]
        sign = np.where((lane // quarter) % 2 == 0, -1.0, 1.0).astype(np.float32)
        for positions, out in ((np.arange(96), rows), (np.arange(64), cols)):
            angle = (positions.astype(np.float32)[:, None] * lane_freq[None, :]).astype(np.float32)
            out.append(np.cos(angle).astype(np.float32))
            out.append((np.sin(angle) * sign).astype(np.float32))
    return np.stack(rows), np.stack(cols)


def place():
    sp, tp = lax.axis_index("sp"), lax.axis_index("tp")
    return sp // NY, sp % NY, tp // NC, tp % NC


def at(z, y, x, c):
    return (z * NY + y, x * NC + c)


def send(src, dst, send_sem, recv_sem, device):
    copy = pltpu.make_async_remote_copy(
        src_ref=src, dst_ref=dst, send_sem=send_sem, recv_sem=recv_sem, device_id=device, device_id_type=MESH
    )
    copy.start()
    return copy


def greet(devices):
    barrier = pltpu.get_barrier_semaphore()
    for device in devices:
        pl.semaphore_signal(barrier, inc=1, device_id=device, device_id_type=MESH)
    pl.semaphore_wait(barrier, len(devices))


def attention_kernel(
    qa, ka, va, qb, kb, gains, rowtab, coltab, outa, outb, resid, norm_gain, gate, up, down,
    mixed_out, normed_out, wall,
    kv, qs, part, parts_in, stat, stats_in, attn, proj, proj_in, sums, sums_in, own_resid,
    kv_send, kv_recv, q_send, q_recv, p_send, p_recv, s_send, s_recv, d_send, d_recv, x_send, x_recv,
    wa_send, wa_recv, wa_local, wz_send, wz_recv, r_sem,
):
    z, y, x, c = place()
    zp, zm = (z + 1) % NZ, (z + NZ - 1) % NZ
    ys = [(y + d) % NY for d in range(NY)]
    xs = [(x + d) % NX for d in range(NX)]
    greet(
        [at(z, ys[d], x, c) for d in (1, 2, 3)]
        + [at(z, ys[d], x, 1 - c) for d in range(4)]
        + [at(z, y, xs[d], c) for d in (1, 2, 3)]
        + [at(zp, y, x, c), at(zm, y, x, c)]
    )

    def near(z_to):
        return at(z_to, y, x, c)

    for h in range(2):
        to_y, to_c = 2 * c + h, y // 2
        mine = jnp.logical_and(to_y == y, to_c == c)
        pieces = [
            (w.at[:, pl.ds(h * HID + t * 128, 128)], wall.at[z, y, g * 3 + t])
            for g, w in enumerate((gate, up))
            for t in range(3)
        ] + [(down.at[h], wall.at[z, y, pl.ds(6, 3)])]

        @pl.when(mine)
        def _():
            for src, dst in pieces:
                pltpu.make_async_copy(src, dst, wa_local).start()

        @pl.when(jnp.logical_not(mine))
        def _():
            for src, dst in pieces:
                send(src, dst, wa_send.at[h], wa_recv.at[y % 2], at(z, to_y, x, to_c))

    rcopy = pltpu.make_async_copy(resid.at[x * NC + c], own_resid, r_sem)
    rcopy.start()

    lane = lax.broadcasted_iota(jnp.int32, (ROWS, 128), 1)
    low = lane < 64

    def table(kind, half):
        sp = z * NY + y
        row = jnp.concatenate(
            [jnp.broadcast_to(rowtab[kind, pl.ds(sp * 3 + r, 1), :], (64, 128)) for r in range(3)], axis=0
        )
        col = jnp.concatenate([coltab[kind]] * 3, axis=0)
        return jnp.where(lane % (2 * half) < half, row, col)

    def turned(v, gain, cos, sin, head):
        quarter = head // 4
        v = v.astype(F32)
        sq = v * v
        if head == 128:
            mean = jnp.sum(sq, axis=-1, keepdims=True) * (1.0 / 128)
        else:
            first = jnp.sum(jnp.where(low, sq, 0.0), axis=-1, keepdims=True)
            second = jnp.sum(jnp.where(low, 0.0, sq), axis=-1, keepdims=True)
            mean = jnp.where(low, first, second) * (1.0 / 64)
        v = v * lax.rsqrt(mean + EPS) * gain
        even = (lane // quarter) % 2 == 0
        other = jnp.where(even, pltpu.roll(v, 128 - quarter, 1), pltpu.roll(v, quarter, 1))
        return v * cos + other * sin

    cos_a, sin_a = table(0, 64), table(1, 64)
    cos_b, sin_b = table(2, 32), table(3, 32)
    kv[z, :, 0:128] = turned(ka[...], gains[1:2, :], cos_a, sin_a, 128).astype(BF16)
    kv[z, :, 128:256] = va[...]
    kb_now = kb[...].astype(F32)
    kv[z, :, 256:384] = jnp.where(low, turned(kb_now, gains[3:4, :], cos_b, sin_b, 64), kb_now).astype(BF16)

    def kv_step(s):
        if s < 4:
            a, b = kv.at[(z + NZ - s + 1) % NZ], kv.at[(z + s - 1) % NZ]
        else:
            a, b = kv.at[(z + 5) % NZ, pl.ds(0, 96)], kv.at[(z + 3) % NZ, pl.ds(96, 96)]
        return (
            send(a, a, kv_send.at[0, s - 1], kv_recv.at[0, s - 1], near(zp)),
            send(b, b, kv_send.at[1, s - 1], kv_recv.at[1, s - 1], near(zm)),
        )

    def w_step(s):
        two = pl.ds(2 * c, 2)
        if s < 4:
            a, b = wall.at[(z + NZ - s + 1) % NZ, two], wall.at[(z + s - 1) % NZ, two]
        else:
            a, b = wall.at[(z + 5) % NZ, pl.ds(2 * c, 1)], wall.at[(z + 3) % NZ, pl.ds(2 * c + 1, 1)]
        return (
            send(a, a, wz_send.at[0, s - 1], wz_recv.at[0, s - 1], near(zp)),
            send(b, b, wz_send.at[1, s - 1], wz_recv.at[1, s - 1], near(zm)),
        )

    def arrived(step):
        for copy in step:
            copy.wait_recv()

    kv_steps = [kv_step(1)]

    for t in range(2):
        qs[y, t] = turned(qa[:, t * 128 : t * 128 + 128], gains[0:1, :], cos_a, sin_a, 128).astype(BF16)
    for t in range(2):
        qs[y, 2 + t] = turned(qb[:, t * 128 : t * 128 + 128], gains[2:3, :], cos_b, sin_b, 64).astype(BF16)
    q_copies = [
        send(qs.at[y], qs.at[y], q_send.at[d - 1], q_recv.at[d - 1], at(z, ys[d], x, c)) for d in (1, 2, 3)
    ]
    for s in (2, 3, 4):
        arrived(kv_steps[-1])
        kv_steps.append(kv_step(s))

    for i in range(2):
        mine = jnp.logical_and(y // 2 == c, y == 2 * c + i)
        whole = wall.at[z, 2 * c + i]

        @pl.when(mine)
        def _():
            pltpu.make_async_copy(whole, whole, wa_local).wait()

        @pl.when(jnp.logical_not(mine))
        def _():
            pltpu.make_async_copy(whole, whole, wa_recv.at[i]).wait()

    w_steps = [w_step(1)]
    arrived(kv_steps[-1])
    for copy in q_copies:
        copy.wait_recv()

    keys = NZ * ROWS
    contract = (((1,), (1,)), ((), ()))

    def one_head(q, key_at, scale):
        k = kv[:, :, key_at : key_at + 128].reshape(keys, 128)
        v = kv[:, :, key_at + (128 if key_at == 0 else 0) : key_at + (256 if key_at == 0 else 128)].reshape(keys, 128)
        score = lax.dot_general(q, k, contract, preferred_element_type=F32)
        top = jnp.max(score, axis=-1, keepdims=True)
        weight = jnp.exp((score - top) * scale)
        total = jnp.sum(weight, axis=-1, keepdims=True)
        blended = jnp.dot(weight.astype(BF16), v, preferred_element_type=F32)
        return blended / total, top * scale + jnp.log(total)

    def attend(yy):
        stats = jnp.zeros((ROWS, 128), F32)
        for t in range(2):
            blended, level = one_head(qs[yy, t], 0, HEAD_A**-0.5)
            part[yy, t] = blended.astype(BF16)
            stats = jnp.where(lane == t, level, stats)
        for t in range(2, 4):
            pair = qs[yy, t].astype(F32)
            first, level1 = one_head(jnp.where(low, pair, 0.0).astype(BF16), 256, HEAD_B**-0.5)
            second, level2 = one_head(jnp.where(low, pltpu.roll(pair, 64, 1), 0.0).astype(BF16), 256, HEAD_B**-0.5)
            part[yy, t] = jnp.where(low, pltpu.roll(first, 64, 1), second).astype(BF16)
            stats = jnp.where(lane == 2 * t - 2, level1, stats)
            stats = jnp.where(lane == 2 * t - 1, level2, stats)
        stat[yy] = jnp.concatenate([stats, stats[0:64]], axis=0).T[0:8, :]

    p_copies = []
    for d in (1, 2, 3, 0):
        attend(ys[d])
        if d:
            p_copies.append(send(part.at[ys[d]], parts_in.at[d - 1], p_send.at[d - 1], p_recv.at[d - 1], at(z, ys[d], x, c)))
            p_copies.append(send(stat.at[ys[d]], stats_in.at[d - 1], s_send.at[d - 1], s_recv.at[d - 1], at(z, ys[d], x, c)))
        if d == 2:
            arrived(w_steps[-1])
            w_steps.append(w_step(2))
    for copy in p_copies:
        copy.wait_recv()

    def columns(block):
        return jnp.concatenate([block, jnp.zeros((120, 256), F32)], axis=0).T[0:ROWS, :]

    levels = [columns(stat[y])] + [columns(stats_in[d]) for d in range(3)]
    best = jnp.maximum(jnp.maximum(levels[0], levels[1]), jnp.maximum(levels[2], levels[3]))
    shares = [jnp.exp(v - best) for v in levels]
    inverse = 1.0 / (shares[0] + shares[1] + shares[2] + shares[3])
    shares = [v * inverse for v in shares]
    for t in range(4):
        total = jnp.zeros((ROWS, 128), F32)
        for d in range(4):
            block = part[y, t] if d == 0 else parts_in[d - 1, t]
            if t < 2:
                share = shares[d][:, t : t + 1]
            else:
                share = jnp.where(low, shares[d][:, 2 * t - 2 : 2 * t - 1], shares[d][:, 2 * t - 1 : 2 * t])
            total = total + share * block.astype(F32)
        attn[:, t * 128 : t * 128 + 128] = total.astype(BF16)

    @pl.loop(0, 8)
    def _(n):
        cols = pl.ds(pl.multiple_of(n * 512, 512), 512)
        acc = jnp.dot(attn[:, 0:256], outa[:, cols], preferred_element_type=F32)
        acc = acc + jnp.dot(attn[:, 256:512], outb[:, cols], preferred_element_type=F32)
        proj[:, :, :, cols] = acc.reshape(NX, NC, OWN, 512).astype(BF16)

    d_copy = send(proj.at[:, 1 - c], proj_in, d_send, d_recv, at(z, y, x, 1 - c))
    arrived(w_steps[-1])
    w_steps.append(w_step(3))
    d_copy.wait_recv()
    x_copies = []
    for d in (2, 1, 3):
        sums[d - 1] = (proj[xs[d], c].astype(F32) + proj_in[xs[d]].astype(F32)).astype(BF16)
        x_copies.append(send(sums.at[d - 1], sums_in.at[d - 1], x_send.at[d - 1], x_recv.at[d - 1], at(z, y, xs[d], c)))
    rcopy.wait()
    mixed_out[...] = own_resid[...].astype(F32) + (proj[x, c].astype(F32) + proj_in[x].astype(F32))
    arrived(w_steps[-1])
    w_steps.append(w_step(4))
    for copy in x_copies:
        copy.wait_recv()
    mixed = mixed_out[...] + sums_in[0].astype(F32) + sums_in[1].astype(F32) + sums_in[2].astype(F32)
    mixed_out[...] = mixed
    mean = jnp.sum(mixed * mixed, axis=-1, keepdims=True) * (1.0 / D)
    normed_out[...] = (mixed * lax.rsqrt(mean + EPS) * norm_gain[...]).astype(BF16)

    arrived(w_steps[-1])
    for step in kv_steps + w_steps:
        for copy in step:
            copy.wait_send()
    for copy in q_copies + p_copies + x_copies + [d_copy]:
        copy.wait_send()
    for h in range(2):
        whole = wall.at[z, y]

        @pl.when(jnp.logical_not(jnp.logical_and(2 * c + h == y, y // 2 == c)))
        def _():
            pltpu.make_async_copy(whole, whole, wa_send.at[h]).wait()


def mixer_kernel(
    normed, mixed, wall,
    out,
    tokens, rows, wgu, wdn, acc, hidden, parts, in1, in2, sum1, sum2, in3, in4,
    g_send, g_recv, h_send, h_recv, w_local, w_send, w_recv, r_send, r_recv, f_send, f_recv, n_sem,
):
    z, y, x, c = place()
    ys = [(y + d) % NY for d in range(NY)]
    xs = [(x + d) % NX for d in range(NX)]
    half = D // 2
    left, right = pl.ds(0, half), pl.ds(half, half)
    to_y = [at(z, ys[d], x, c) for d in range(4)]
    to_x = [at(z, y, xs[d], c) for d in range(4)]
    other = at(z, y, x, 1 - c)
    ncopy = pltpu.make_async_copy(normed, tokens.at[y, x], n_sem)
    ncopy.start()
    greet(to_y[1:] + to_x[1:] + [other])

    first = []
    for d in (2, 1, 3):
        first.append(send(normed.at[:, left], tokens.at[y, x, :, left], g_send.at[0, d - 1], g_recv.at[0, d - 1], to_x[d]))
        first.append(send(normed.at[:, right], tokens.at[y, x, :, right], g_send.at[1, d - 1], g_recv.at[1, d - 1], to_y[d]))

    two = pl.ds(2 * c, 2)
    pieces = [(wall.at[:, two, t], wgu.at[:, two, :, pl.ds(t * 128, 128)]) for t in range(6)] + [
        (wall.at[zz, 2 * c + i, pl.ds(6, 3)], wdn.at[:, :, pl.ds(pl.multiple_of((zz * NY + 2 * c + i) * 128, 128), 128)])
        for zz in range(NZ)
        for i in range(2)
    ]
    for src, dst in pieces:
        pltpu.make_async_copy(src, dst, w_local).start()
        send(src, dst, w_send, w_recv, other)

    for copy in first:
        copy.wait_recv()
    ncopy.wait()
    second = []
    for d in (2, 1, 3):
        mine = tokens.at[y, :, :, left]
        second.append(send(mine, mine, h_send.at[0, d - 1], h_recv.at[0, d - 1], to_y[d]))
        mine = tokens.at[:, x, :, right]
        second.append(send(mine, mine, h_send.at[1, d - 1], h_recv.at[1, d - 1], to_x[d]))

    got = wall.at[:, two]
    pltpu.make_async_copy(got, got, w_local).wait()
    pltpu.make_async_copy(got, got, w_recv).wait()
    for copy in second:
        copy.wait_recv()

    count = NY * NX * OWN

    @pl.loop(0, 8)
    def _(n):
        cols = pl.ds(pl.multiple_of(n * 512, 512), 512)
        block = tokens[:, :, :, cols].astype(F32).reshape(count, 512)
        block = block.astype(BF16)
        weights = wgu[pl.ds(n, 1)].reshape(512, 2 * HID)
        now = jnp.dot(block, weights, preferred_element_type=F32)

        @pl.when(n == 0)
        def _():
            acc[...] = now

        @pl.when(n > 0)
        def _():
            acc[...] += now

    gate = acc[:, 0:HID]
    hidden[...] = (gate / (1.0 + jnp.exp(-gate)) * acc[:, HID : 2 * HID]).astype(BF16)

    @pl.loop(0, 8)
    def _(n):
        cols = pl.ds(pl.multiple_of(n * 512, 512), 512)
        now = jnp.dot(hidden[...], wdn[:, :, cols].reshape(HID, 512), preferred_element_type=F32)
        parts[:, :, :, cols] = now.reshape(NY, NX, OWN, 512).astype(BF16)

    third = []
    for d in (2, 1, 3):
        third.append(send(parts.at[ys[d], :, :, left], in1.at[d - 1], r_send.at[0, d - 1], r_recv.at[0, d - 1], to_y[d]))
        third.append(send(parts.at[:, xs[d], :, right], in2.at[d - 1], r_send.at[1, d - 1], r_recv.at[1, d - 1], to_x[d]))
    for copy in third:
        copy.wait_recv()
    fourth = []
    for d in (2, 1, 3, 0):
        total = parts[y, xs[d], :, 0:half].astype(F32)
        for e in range(3):
            total = total + in1[e, xs[d]].astype(F32)
        if d:
            sum1[d - 1] = total.astype(BF16)
            fourth.append(send(sum1.at[d - 1], in3.at[d - 1], f_send.at[0, d - 1], f_recv.at[0, d - 1], to_x[d]))
        else:
            acc1 = total
        total = parts[ys[d], x, :, half:D].astype(F32)
        for e in range(3):
            total = total + in2[e, ys[d]].astype(F32)
        if d:
            sum2[d - 1] = total.astype(BF16)
            fourth.append(send(sum2.at[d - 1], in4.at[d - 1], f_send.at[1, d - 1], f_recv.at[1, d - 1], to_y[d]))
        else:
            acc2 = total
    for copy in fourth:
        copy.wait_recv()
    for e in range(3):
        acc1 = acc1 + in3[e].astype(F32)
        acc2 = acc2 + in4[e].astype(F32)
    out[:, 0:half] = (mixed[:, 0:half] + 0.5 * acc1).astype(BF16)
    out[:, half:D] = (mixed[:, half:D] + 0.5 * acc2).astype(BF16)
    for copy in first + second + third + fourth:
        copy.wait_send()
    pltpu.make_async_copy(got, got, w_send).wait()


VM = pl.BlockSpec(memory_space=pltpu.VMEM)
ANY = pl.BlockSpec(memory_space=pl.ANY)
DMA = pltpu.SemaphoreType.DMA


def on_device(
    query_a, key_a, value_a, query_b, key_b, value_b, gain_a, gain_b, out_a, out_b, residual, norm_gain,
    gate_weight, up_weight, down_weight,
):
    rowtab, coltab = turn_tables()
    gains = jnp.concatenate([gain_a, jnp.concatenate([gain_b, gain_b], axis=1)], axis=0)
    keys_b = jnp.concatenate([key_b, value_b], axis=1)
    mixed, normed, wall = pl.pallas_call(
        attention_kernel,
        out_shape=(
            jax.ShapeDtypeStruct((OWN, D), F32),
            jax.ShapeDtypeStruct((OWN, D), BF16),
            jax.ShapeDtypeStruct((NZ, NY, 9, 128, 128), BF16),
        ),
        in_specs=[VM] * 10 + [ANY] + [VM] * 4,
        out_specs=(VM, VM, ANY),
        scratch_shapes=[
            pltpu.VMEM((NZ, ROWS, 384), BF16),
            pltpu.VMEM((NY, 4, ROWS, 128), BF16),
            pltpu.VMEM((NY, 4, ROWS, 128), BF16),
            pltpu.VMEM((3, 4, ROWS, 128), BF16),
            pltpu.VMEM((NY, 8, 256), F32),
            pltpu.VMEM((3, 8, 256), F32),
            pltpu.VMEM((ROWS, 512), BF16),
            pltpu.VMEM((NX, NC, OWN, D), BF16),
            pltpu.VMEM((NX, OWN, D), BF16),
            pltpu.VMEM((3, OWN, D), BF16),
            pltpu.VMEM((3, OWN, D), BF16),
            pltpu.VMEM((OWN, D), BF16),
            DMA((2, 4)), DMA((2, 4)), DMA((3,)), DMA((3,)), DMA((3,)), DMA((3,)), DMA((3,)), DMA((3,)),
            DMA, DMA, DMA((3,)), DMA((3,)),
            DMA((2,)), DMA((2,)), DMA, DMA((2, 4)), DMA((2, 4)), DMA,
        ],
        compiler_params=pltpu.CompilerParams(collective_id=0, has_side_effects=True, vmem_limit_bytes=60 * 2**20),
        name="attend",
    )(
        query_a, key_a, value_a, query_b, keys_b, gains, jnp.asarray(rowtab), jnp.asarray(coltab), out_a, out_b,
        residual.reshape(NX * NC, OWN, D), norm_gain.reshape(1, D), gate_weight, up_weight,
        down_weight.reshape(2, 3, 128, 128),
    )
    half = D // 2
    return pl.pallas_call(
        mixer_kernel,
        out_shape=jax.ShapeDtypeStruct((OWN, D), BF16),
        in_specs=[VM, VM, ANY],
        out_specs=VM,
        scratch_shapes=[
            pltpu.VMEM((NY, NX, OWN, D), BF16),
            pltpu.VMEM((8, 128), BF16),
            pltpu.VMEM((NZ, NY, 128, 2 * HID), BF16),
            pltpu.VMEM((3, 128, D), BF16),
            pltpu.VMEM((NY * NX * OWN, 2 * HID), F32),
            pltpu.VMEM((NY * NX * OWN, HID), BF16),
            pltpu.VMEM((NY, NX, OWN, D), BF16),
            pltpu.VMEM((3, NX, OWN, half), BF16),
            pltpu.VMEM((3, NY, OWN, half), BF16),
            pltpu.VMEM((3, OWN, half), BF16),
            pltpu.VMEM((3, OWN, half), BF16),
            pltpu.VMEM((3, OWN, half), BF16),
            pltpu.VMEM((3, OWN, half), BF16),
            DMA((2, 3)), DMA((2, 3)), DMA((2, 3)), DMA((2, 3)), DMA, DMA, DMA,
            DMA((2, 3)), DMA((2, 3)), DMA((2, 3)), DMA((2, 3)), DMA,
        ],
        compiler_params=pltpu.CompilerParams(collective_id=1, has_side_effects=True, vmem_limit_bytes=60 * 2**20),
        name="mixer",
    )(normed, mixed, wall)


def solution(mesh):
    return jax.shard_map(
        on_device,
        mesh=mesh,
        in_specs=(
            P("sp", "tp"), P("sp", "tp"), P("sp", "tp"), P("sp", "tp"), P("sp", "tp"), P("sp", "tp"),
            P(), P(), P("tp", None), P("tp", None), P("sp", None), P(),
            P("sp", "tp"), P("sp", "tp"), P("tp", "sp"),
        ),
        out_specs=P(("sp", "tp"), None),
        check_vma=False,
    )
```

time: 316 us -> 146 us (0.46)
  waiting for transfers between devices: 163 us -> 0 us
  Pallas kernels: 0 us -> 141 us
  blocking collectives: 53.4 us -> 0 us
  matrix products: 43.4 us -> 0 us
  other arithmetic: 25.2 us -> 2.15 us
  between operations: 13.8 us -> 0.02 us
  starting transfers between devices: 9.09 us -> 0 us
  local copies, waits for them, and re-layouts: 6.82 us -> 3.36 us
    all_gather x2 -> x0, waiting for transfers between devices: 143 us -> none  [the longest x1 77.9 us: side_by_side(): filled = lax.all_gather(both, axis, axis=dim, tiled=True)]
    pallas_call x0 -> x2, Pallas kernels: none -> 141 us  [the longest x1 78.1 us: on_device(): pl.pallas_call(attention_kernel, out_shape=(jax.ShapeDtypeStruct((OWN, D)...]
    all_to_all x2 -> x0, blocking collectives: 53.4 us -> none  [the longest x1 28.8 us: sum_at_owner(): lax.all_to_all(parts, axis, split_axis=0, concat_axis=0, tiled=True)]
    dot_general x8 -> x0, matrix products: 43.4 us -> none  [the longest x2 12.1 us: attend(): jnp.einsum('kgtp,pkd->kgtd', exp_scores.astype(jnp.bfloat16), v_heads, pr...]
    all_to_all x1 -> x0, waiting for transfers between devices: 20.6 us -> none  [sum_at_owner(): lax.all_to_all(parts, axis, split_axis=0, concat_axis=0, tiled=True)]
    reduce_sum x9 -> x0, other arithmetic: 14.4 us -> none  [the longest x2 11.1 us: attend(): new_sum = jnp.sum(exp_scores, axis=-1)]
    all_to_all x1 -> x0, starting transfers between devices: 9.04 us -> none  [sum_at_owner(): lax.all_to_all(parts, axis, split_axis=0, concat_axis=0, tiled=True)]
    convert_element_type x6 -> x0, other arithmetic: 4.26 us -> none  [the longest x1 1.7 us: on_device(): return (mixed_rows + 0.5 * branch_sum).astype(jnp.bfloat16)]
  transfers between devices with their start and end apart: 3 -> 0, of which waited for: 3 -> 0; matrix products, arithmetic and copies ran while one was open for 15% -> 0% of each run, Pallas kernels for 0% -> 0%
where the time goes in v1:
time: 146 us
  Pallas kernels  141 us (97%)
  local copies, waits for them, and re-layouts  3.36 us (2%)
  other arithmetic  2.15 us (1%)
    pallas_call x1, Pallas kernels, on_device(): pl.pallas_call(attention_kernel, out_shape=(jax.ShapeDtypeStruct((OWN, D)...  78.1 us
    pallas_call x1, Pallas kernels, on_device(): pl.pallas_call(mixer_kernel, out_shape=jax.ShapeDtypeStruct((OWN, D), BF1...  62.5 us
    unnamed x3, local copies, waits for them, and re-layouts  3.36 us

profile of v1, /device:TPU:1, one launch (start us, length us, event | category | flops | bytes accessed | tf_op | source)
XLA Modules:
  0.0 146.2 jit_solution(8611658084853901146)
XLA Ops:
  0.0 1.4 maximum_maximum_fusion.gains
  1.4 0.9 copy.18
  2.3 0.9 copy.19
  3.2 0.7 pad_maximum_fusion.kb
  3.9 78.1 %attend.1 = (f32[24,4096]{1,0:T(8,128)}, bf16[24,4096]{1,0:T(8,128)(2,1)}, bf16[8,4,9,128,128]{4,3,2,1,0:T(8,128)(2,1)}) custom-call(bf16[192,256]{1,0:T(8,128)(2,1)} %qa.1, bf16[192,128]{1,0:T(8,128)(2,1)} %ka.1, bf16[192,128]{1,0:T(8,128)(2,1)} %va.1, bf16[192,256]{1,0:T(8,128)(2,1)} %qb.1, bf16[192,128]{1,0:T(8,128)(2,1)} %pad_maximum_fusion.kb, ...), custom_call_target="tpu_custom_call" | custom-call | tf_op jit(solution)/shard_map/attend/pallas_call | solution.py:414
  82.0 62.5 %mixer.1 = bf16[24,4096]{1,0:T(8,128)(2,1)} custom-call(bf16[24,4096]{1,0:T(8,128)(2,1)} %get-tuple-element.8.normed, f32[24,4096]{1,0:T(8,128)} %get-tuple-element.9.mixed, bf16[8,4,9,128,128]{4,3,2,1,0:T(8,128)(2,1)} %get-tuple-element.10.wall), custom_call_target="tpu_custom_call" | custom-call | tf_op jit(solution)/shard_map/mixer/pallas_call | solution.py:448
  144.5 1.6 %copy.21 = bf16[24,4096]{1,0:T(8,128)(2,1)} copy(bf16[24,4096]{1,0:T(8,128)(2,1)} %mixer.1) | data formatting | bytes 393216

commit v2 on v1

v2 whole, which is shorter than its diff:
```python
import jax
import jax.numpy as jnp
import numpy as np
from jax import lax
from jax.experimental import pallas as pl
from jax.experimental.pallas import tpu as pltpu
from jax.sharding import PartitionSpec as P

NZ, NY, NX, NC = 8, 4, 4, 2
ROWS = 192
OWN = 24
HEAD_A, HEAD_B, GRID_W = 128, 64, 64
D = 4096
HID = 384
EPS = 1e-06
BASE = 10000.0
MESH = pl.DeviceIdType.MESH
F32, BF16 = jnp.float32, jnp.bfloat16


def turn_tables():
    rows, cols = [], []
    for head in (HEAD_A, HEAD_B):
        quarter = head // 4
        freq = np.float32(BASE) ** (-4.0 * np.arange(quarter, dtype=np.float32) / head).astype(np.float32)
        lane = np.arange(128)
        lane_freq = freq[lane % quarter]
        sign = np.where((lane // quarter) % 2 == 0, -1.0, 1.0).astype(np.float32)
        for positions, out in ((np.arange(96), rows), (np.arange(64), cols)):
            angle = (positions.astype(np.float32)[:, None] * lane_freq[None, :]).astype(np.float32)
            out.append(np.cos(angle).astype(np.float32))
            out.append((np.sin(angle) * sign).astype(np.float32))
    return np.stack(rows), np.stack(cols)


def place():
    sp, tp = lax.axis_index("sp"), lax.axis_index("tp")
    return sp // NY, sp % NY, tp // NC, tp % NC


def at(z, y, x, c):
    return (z * NY + y, x * NC + c)


def send(src, dst, send_sem, recv_sem, device):
    copy = pltpu.make_async_remote_copy(
        src_ref=src, dst_ref=dst, send_sem=send_sem, recv_sem=recv_sem, device_id=device, device_id_type=MESH
    )
    copy.start()
    return copy


def greet(devices):
    barrier = pltpu.get_barrier_semaphore()
    for device in devices:
        pl.semaphore_signal(barrier, inc=1, device_id=device, device_id_type=MESH)
    pl.semaphore_wait(barrier, len(devices))


HEADS = 6
LOG2E = 1.4426950408889634
SLOT = {0: 0, 1: 1, -1: 2, 2: 3, -2: 4, 3: 5, -3: 6, 4: 7}
EARLY = 5 * ROWS


def layer_kernel(
    qa, ka, va, qb, kb, vb, gain_a, gain_b, rowtab, coltab, outa_any, outb_any, resid, norm_gain, gate, up, down,
    out,
    kv, qs, qx, run_acc, run_stat, part, parts_in, stat, stats_in, attn, outa, outb, proj, proj_in, sums, sums_in,
    own_resid, mixed, normed, tokens, wgu, wdn, acc, hidden, parts, in1, in2, sum1, sum2, in3, in4,
    kv_send, kv_recv, q_send, q_recv, p_send, p_recv, s_send, s_recv, d_send, d_recv, x_send, x_recv,
    wa_send, wa_recv, wa_local, wz_send, wz_recv, wc_send, wc_recv, r_sem, o_sem,
    g_send, g_recv, h_send, h_recv, t_send, t_recv, f_send, f_recv,
):
    z, y, x, c = place()
    ys = [(y + d) % NY for d in range(NY)]
    xs = [(x + d) % NX for d in range(NX)]
    to_y = [at(z, ys[d], x, c) for d in range(NY)]
    to_x = [at(z, y, xs[d], c) for d in range(NX)]
    up_z, down_z = at((z + 1) % NZ, y, x, c), at((z + NZ - 1) % NZ, y, x, c)
    other = at(z, y, x, 1 - c)

    loads = [
        pltpu.make_async_copy(resid.at[x * NC + c], own_resid, r_sem),
        pltpu.make_async_copy(outa_any, outa, o_sem.at[0]),
        pltpu.make_async_copy(outb_any, outb, o_sem.at[1]),
    ]
    for copy in loads:
        copy.start()

    lane = lax.broadcasted_iota(jnp.int32, (ROWS, 128), 1)
    low = lane < 64

    def table(kind, half):
        sp = z * NY + y
        row = jnp.concatenate(
            [jnp.broadcast_to(rowtab[kind, pl.ds(sp * 3 + r, 1), :], (64, 128)) for r in range(3)], axis=0
        )
        col = jnp.concatenate([coltab[kind]] * 3, axis=0)
        return jnp.where(lane % (2 * half) < half, row, col)

    def turned(v, gain, cos, sin, head):
        quarter = head // 4
        v = v.astype(F32)
        sq = v * v
        if head == 128:
            mean = jnp.sum(sq, axis=-1, keepdims=True) * (1.0 / 128)
        else:
            first = jnp.sum(jnp.where(low, sq, 0.0), axis=-1, keepdims=True)
            second = jnp.sum(jnp.where(low, 0.0, sq), axis=-1, keepdims=True)
            mean = jnp.where(low, first, second) * (1.0 / 64)
        v = v * lax.rsqrt(mean + EPS) * gain
        even = (lane // quarter) % 2 == 0
        rolled = jnp.where(even, pltpu.roll(v, 128 - quarter, 1), pltpu.roll(v, quarter, 1))
        return v * cos + rolled * sin

    def twice(v):
        return jnp.concatenate([v, v], axis=-1)

    cos_a, sin_a = table(0, 64), table(1, 64)
    cos_b, sin_b = table(2, 32), table(3, 32)
    kv[0, :, 0:128] = turned(ka[...], gain_a[1:2, :], cos_a, sin_a, 128).astype(BF16)
    kv[0, :, 128:256] = va[...]
    kb_now = jnp.concatenate([kb[...].astype(F32), vb[...].astype(F32)], axis=0).T
    kv[0, :, 256:384] = jnp.where(low, turned(kb_now, twice(gain_b[1:2, :]), cos_b, sin_b, 64), kb_now).astype(BF16)

    for t in range(2):
        qs[0, t] = turned(qa[:, t * 128 : t * 128 + 128], gain_a[0:1, :], cos_a, sin_a, 128).astype(BF16)
    for t in range(2):
        qs[0, 2 + t] = turned(qb[:, t * 128 : t * 128 + 128], twice(gain_b[0:1, :]), cos_b, sin_b, 64).astype(BF16)
    greet(to_y[1:] + [at(z, ys[d], x, 1 - c) for d in range(4)] + to_x[1:] + [up_z, down_z])

    def kv_step(s):
        rows = (pl.ds(0, ROWS), pl.ds(0, ROWS)) if s < 4 else (pl.ds(0, 96), pl.ds(96, 96))
        return [
            send(
                kv.at[SLOT[sign * (s - 1)], rows[k]], kv.at[SLOT[sign * s] if s < 4 else 7, rows[k]],
                kv_send.at[k, s - 1], kv_recv.at[k, s - 1], (up_z, down_z)[k],
            )
            for k, sign in ((0, -1), (1, 1))
        ]

    def arrived(copies):
        for copy in copies:
            copy.wait_recv()

    kv_steps = [kv_step(1)]
    q_copies = [send(qs.at[0], qs.at[(4 - d) % 4], q_send.at[d - 1], q_recv.at[d - 1], to_y[d]) for d in (2, 1, 3)]

    def down_cols(zz, yy, count):
        return wdn.at[:, :, pl.ds(pl.multiple_of((zz * NY + yy) * 128, 128), count * 128)]

    def first_pieces(h):
        return [
            (gate.at[:, pl.ds(h * HID, HID)], wgu.at[z, y, :, pl.ds(0, HID)]),
            (up.at[:, pl.ds(h * HID, HID)], wgu.at[z, y, :, pl.ds(HID, HID)]),
            (down.at[h], down_cols(z, y, 1)),
        ]

    def stays(h):
        return jnp.logical_and(2 * c + h == y, y // 2 == c)

    for h in range(2):

        @pl.when(stays(h))
        def _():
            for i, (src, dst) in enumerate(first_pieces(h)):
                pltpu.make_async_copy(src, dst, wa_local.at[i]).start()

        @pl.when(jnp.logical_not(stays(h)))
        def _():
            for i, (src, dst) in enumerate(first_pieces(h)):
                send(src, dst, wa_send.at[h, i], wa_recv.at[y % 2, i], at(z, 2 * c + h, x, y // 2))

    def w_pieces(zz, start, count):
        return [wgu.at[zz, pl.ds(start, count)], down_cols(zz, start, count)]

    def w_step(s):
        if s < 4:
            refs = [w_pieces((z + NZ - s + 1) % NZ, 2 * c, 2), w_pieces((z + s - 1) % NZ, 2 * c, 2)]
        else:
            refs = [w_pieces((z + 5) % NZ, 2 * c, 1), w_pieces((z + 3) % NZ, 2 * c + 1, 1)]
        return [
            send(ref, ref, wz_send.at[k, s - 1, i], wz_recv.at[k, s - 1, i], (up_z, down_z)[k])
            for k in range(2)
            for i, ref in enumerate(refs[k])
        ]

    def w_across(index, zz):
        return [
            send(ref, ref, wc_send.at[index, i], wc_recv.at[index, i], other)
            for i, ref in enumerate(w_pieces(zz, 2 * c, 2))
        ]

    arrived(kv_steps[-1])
    kv_steps.append(kv_step(2))
    arrived(kv_steps[-1])
    kv_steps.append(kv_step(3))
    arrived(q_copies)

    contract = (((1,), (1,)), ((), ()))

    def piece(q, k, v, scale):
        score = lax.dot_general(q, k, contract, preferred_element_type=F32)
        top = jnp.max(score, axis=-1, keepdims=True)
        weight = jnp.exp2((score - top) * (scale * LOG2E))
        total = jnp.sum(weight, axis=-1, keepdims=True)
        return top * (scale * LOG2E), total, jnp.dot(weight.astype(BF16), v, preferred_element_type=F32)

    def group_a(yy, slots, count):
        k = kv[slots, :, 0:128].reshape(count, 128)
        v = kv[slots, :, 128:256].reshape(count, 128)
        return piece(qs[yy, 0:2].reshape(2 * ROWS, 128), k, v, HEAD_A**-0.5)

    def group_b(yy, slots, count):
        k = kv[slots, :, 256:384].reshape(count, 128)
        return piece(qx[yy].reshape(4 * ROWS, 128), k, k, HEAD_B**-0.5)

    def noted(tops, totals, top, total, start, count):
        for j in range(count):
            rows = slice(j * ROWS, j * ROWS + ROWS)
            tops = jnp.where(lane == start + j, top[rows], tops)
            totals = jnp.where(lane == start + j, total[rows], totals)
        return tops, totals

    def early(yy):
        for t in range(2):
            pair = qs[yy, 2 + t].astype(F32)
            qx[yy, 2 * t] = jnp.where(low, pair, 0.0).astype(BF16)
            qx[yy, 2 * t + 1] = jnp.where(low, pltpu.roll(pair, 64, 1), 0.0).astype(BF16)
        tops, totals = jnp.zeros((ROWS, 128), F32), jnp.ones((ROWS, 128), F32)
        for start, count, group in ((0, 2, group_a), (2, 4, group_b)):
            top, total, blended = group(yy, slice(0, 5), EARLY)
            run_acc[yy, start : start + count] = blended.reshape(count, ROWS, 128)
            tops, totals = noted(tops, totals, top, total, start, count)
        run_stat[yy, 0] = tops
        run_stat[yy, 1] = totals

    def late(yy):
        tops, totals, blends = jnp.zeros((ROWS, 128), F32), jnp.ones((ROWS, 128), F32), []
        for start, count, group in ((0, 2, group_a), (2, 4, group_b)):
            top, total, blended = group(yy, slice(5, 8), 3 * ROWS)
            tops, totals = noted(tops, totals, top, total, start, count)
            blends += [blended[j * ROWS : j * ROWS + ROWS] for j in range(count)]
        best = jnp.maximum(run_stat[yy, 0], tops)
        share0, share1 = jnp.exp2(run_stat[yy, 0] - best), jnp.exp2(tops - best)
        all_total = share0 * run_stat[yy, 1] + share1 * totals
        inverse = 1.0 / all_total
        share0, share1 = share0 * inverse, share1 * inverse
        done = [
            share0[:, j : j + 1] * run_acc[yy, j] + share1[:, j : j + 1] * blends[j] for j in range(HEADS)
        ]
        stats = best + jnp.log2(all_total)
        part[yy, 0] = done[0].astype(BF16)
        part[yy, 1] = done[1].astype(BF16)
        for t in range(2):
            part[yy, 2 + t] = jnp.where(low, pltpu.roll(done[2 + 2 * t], 64, 1), done[3 + 2 * t]).astype(BF16)
        stat[yy] = jnp.concatenate([stats, stats[0:64]], axis=0).T[0:8, :]

    def p_send_to(d):
        return [
            send(part.at[d], parts_in.at[d - 1], p_send.at[d - 1], p_recv.at[d - 1], to_y[d]),
            send(stat.at[d], stats_in.at[d - 1], s_send.at[d - 1], s_recv.at[d - 1], to_y[d]),
        ]

    pl.loop(0, 2)(early)
    arrived(kv_steps[-1])
    kv_steps.append(kv_step(4))
    for i in range(2):
        landing = [wgu.at[z, 2 * c + i, :, pl.ds(0, HID)], wgu.at[z, 2 * c + i, :, pl.ds(HID, HID)], down_cols(z, 2 * c + i, 1)]
        home = jnp.logical_and(y // 2 == c, y == 2 * c + i)

        @pl.when(home)
        def _():
            for j, ref in enumerate(landing):
                pltpu.make_async_copy(ref, ref, wa_local.at[j]).wait()

        @pl.when(jnp.logical_not(home))
        def _():
            for j, ref in enumerate(landing):
                pltpu.make_async_copy(ref, ref, wa_recv.at[i, j]).wait()

    w_steps = [w_step(1)]
    across = w_across(0, z)
    pl.loop(2, 4)(early)
    arrived(kv_steps[-1])
    p_copies = []
    for d in (2, 1, 3, 0):
        late(d)
        if d:
            p_copies += p_send_to(d)
    arrived(w_steps[-1])
    w_steps.append(w_step(2))
    across += w_across(1, (z + NZ - 1) % NZ) + w_across(2, (z + 1) % NZ)
    arrived(p_copies)

    def columns(block):
        return jnp.concatenate([block, jnp.zeros((120, 256), F32)], axis=0).T[0:ROWS, :]

    levels = [columns(stat[0])] + [columns(stats_in[d]) for d in range(3)]
    best = jnp.maximum(jnp.maximum(levels[0], levels[1]), jnp.maximum(levels[2], levels[3]))
    shares = [jnp.exp2(v - best) for v in levels]
    inverse = 1.0 / (shares[0] + shares[1] + shares[2] + shares[3])
    shares = [v * inverse for v in shares]
    for t in range(4):
        total = jnp.zeros((ROWS, 128), F32)
        for d in range(4):
            block = part[0, t] if d == 0 else parts_in[d - 1, t]
            if t < 2:
                share = shares[d][:, t : t + 1]
            else:
                share = jnp.where(low, shares[d][:, 2 * t - 2 : 2 * t - 1], shares[d][:, 2 * t - 1 : 2 * t])
            total = total + share * block.astype(F32)
        attn[:, t * 128 : t * 128 + 128] = total.astype(BF16)

    for copy in loads:
        copy.wait()

    @pl.loop(0, 8)
    def _(n):
        cols = pl.ds(pl.multiple_of(n * 512, 512), 512)
        now = jnp.dot(attn[:, 0:256], outa[:, cols], preferred_element_type=F32)
        now = now + jnp.dot(attn[:, 256:512], outb[:, cols], preferred_element_type=F32)
        proj[:, :, :, cols] = now.reshape(NX, NC, OWN, 512).astype(BF16)

    d_copy = send(proj.at[:, 1 - c], proj_in, d_send, d_recv, other)
    d_copy.wait_recv()
    x_copies = []
    for d in (2, 1, 3):
        sums[d - 1] = (proj[xs[d], c].astype(F32) + proj_in[xs[d]].astype(F32)).astype(BF16)
        x_copies.append(send(sums.at[d - 1], sums_in.at[d - 1], x_send.at[d - 1], x_recv.at[d - 1], to_x[d]))
    mixed[...] = own_resid[...].astype(F32) + (proj[x, c].astype(F32) + proj_in[x].astype(F32))
    arrived(w_steps[-1])
    w_steps.append(w_step(3))
    across += w_across(3, (z + NZ - 2) % NZ) + w_across(4, (z + 2) % NZ)
    arrived(x_copies)
    total = mixed[...] + sums_in[0].astype(F32) + sums_in[1].astype(F32) + sums_in[2].astype(F32)
    mixed[...] = total
    mean = jnp.sum(total * total, axis=-1, keepdims=True) * (1.0 / D)
    normed[...] = (total * lax.rsqrt(mean + EPS) * norm_gain[...]).astype(BF16)
    tokens[0, 0] = normed[...]

    half = D // 2
    left, right = pl.ds(0, half), pl.ds(half, half)
    first = []
    for d in (2, 1, 3):
        first.append(send(normed.at[:, left], tokens.at[0, 4 - d, :, left], g_send.at[0, d - 1], g_recv.at[0, d - 1], to_x[d]))
        first.append(send(normed.at[:, right], tokens.at[4 - d, 0, :, right], g_send.at[1, d - 1], g_recv.at[1, d - 1], to_y[d]))
    arrived(first)
    second = []
    for d in (2, 1, 3):
        second.append(
            send(tokens.at[0, :, :, left], tokens.at[4 - d, :, :, left], h_send.at[0, d - 1], h_recv.at[0, d - 1], to_y[d])
        )
        second.append(
            send(tokens.at[:, 0, :, right], tokens.at[:, 4 - d, :, right], h_send.at[1, d - 1], h_recv.at[1, d - 1], to_x[d])
        )
    arrived(w_steps[-1])
    w_steps.append(w_step(4))
    across += w_across(5, (z + NZ - 3) % NZ) + w_across(6, (z + 3) % NZ)
    arrived(w_steps[-1])
    across += w_across(7, (z + 4) % NZ)
    arrived(second)
    arrived(across)

    count = NY * NX * OWN

    @pl.loop(0, 8)
    def _(n):
        cols = pl.ds(pl.multiple_of(n * 512, 512), 512)
        block = tokens[:, :, :, cols].astype(F32).reshape(count, 512).astype(BF16)
        now = jnp.dot(block, wgu[pl.ds(n, 1)].reshape(512, 2 * HID), preferred_element_type=F32)

        @pl.when(n == 0)
        def _():
            acc[...] = now

        @pl.when(n > 0)
        def _():
            acc[...] += now

    gated = acc[:, 0:HID]
    hidden[...] = (gated / (1.0 + jnp.exp(-gated)) * acc[:, HID : 2 * HID]).astype(BF16)

    @pl.loop(0, 8)
    def _(n):
        cols = pl.ds(pl.multiple_of(n * 512, 512), 512)
        now = jnp.dot(hidden[...], wdn[:, :, cols].reshape(HID, 512), preferred_element_type=F32)
        parts[:, :, :, cols] = now.reshape(NY, NX, OWN, 512).astype(BF16)

    third = []
    for d in (2, 1, 3):
        third.append(send(parts.at[d, :, :, left], in1.at[d - 1], t_send.at[0, d - 1], t_recv.at[0, d - 1], to_y[d]))
        third.append(send(parts.at[:, d, :, right], in2.at[d - 1], t_send.at[1, d - 1], t_recv.at[1, d - 1], to_x[d]))
    arrived(third)
    fourth = []
    for d in (2, 1, 3, 0):
        total1 = parts[0, d, :, 0:half].astype(F32)
        total2 = parts[d, 0, :, half:D].astype(F32)
        for e in range(3):
            total1 = total1 + in1[e, d].astype(F32)
            total2 = total2 + in2[e, d].astype(F32)
        if d:
            sum1[d - 1] = total1.astype(BF16)
            fourth.append(send(sum1.at[d - 1], in3.at[d - 1], f_send.at[0, d - 1], f_recv.at[0, d - 1], to_x[d]))
            sum2[d - 1] = total2.astype(BF16)
            fourth.append(send(sum2.at[d - 1], in4.at[d - 1], f_send.at[1, d - 1], f_recv.at[1, d - 1], to_y[d]))
    arrived(fourth)
    for e in range(3):
        total1 = total1 + in3[e].astype(F32)
        total2 = total2 + in4[e].astype(F32)
    out[:, 0:half] = (mixed[:, 0:half] + 0.5 * total1).astype(BF16)
    out[:, half:D] = (mixed[:, half:D] + 0.5 * total2).astype(BF16)

    for copy in sum(kv_steps, []) + q_copies + sum(w_steps, []) + across + p_copies + [d_copy] + x_copies:
        copy.wait_send()
    for copy in first + second + third + fourth:
        copy.wait_send()
    for h in range(2):

        @pl.when(jnp.logical_not(stays(h)))
        def _():
            for i, (src, dst) in enumerate(first_pieces(h)):
                pltpu.make_async_copy(dst, dst, wa_send.at[h, i]).wait()


VM = pl.BlockSpec(memory_space=pltpu.VMEM)
ANY = pl.BlockSpec(memory_space=pl.ANY)
DMA = pltpu.SemaphoreType.DMA


def on_device(
    query_a, key_a, value_a, query_b, key_b, value_b, gain_a, gain_b, out_a, out_b, residual, norm_gain,
    gate_weight, up_weight, down_weight,
):
    rowtab, coltab = turn_tables()
    half = D // 2
    vmem = pltpu.VMEM
    return pl.pallas_call(
        layer_kernel,
        out_shape=jax.ShapeDtypeStruct((OWN, D), BF16),
        in_specs=[VM] * 10 + [ANY] * 3 + [VM] + [ANY] * 3,
        out_specs=VM,
        scratch_shapes=[
            vmem((NZ, ROWS, 384), BF16),
            vmem((NY, 4, ROWS, 128), BF16),
            vmem((NY, 4, ROWS, 128), BF16),
            vmem((NY, HEADS, ROWS, 128), F32),
            vmem((NY, 2, ROWS, 128), F32),
            vmem((NY, 4, ROWS, 128), BF16),
            vmem((3, 4, ROWS, 128), BF16),
            vmem((NY, 8, 256), F32),
            vmem((3, 8, 256), F32),
            vmem((ROWS, 512), BF16),
            vmem((256, D), BF16),
            vmem((256, D), BF16),
            vmem((NX, NC, OWN, D), BF16),
            vmem((NX, OWN, D), BF16),
            vmem((3, OWN, D), BF16),
            vmem((3, OWN, D), BF16),
            vmem((OWN, D), BF16),
            vmem((OWN, D), F32),
            vmem((OWN, D), BF16),
            vmem((NY, NX, OWN, D), BF16),
            vmem((NZ, NY, 128, 2 * HID), BF16),
            vmem((3, 128, D), BF16),
            vmem((NY * NX * OWN, 2 * HID), F32),
            vmem((NY * NX * OWN, HID), BF16),
            vmem((NY, NX, OWN, D), BF16),
            vmem((3, NX, OWN, half), BF16),
            vmem((3, NY, OWN, half), BF16),
            vmem((3, OWN, half), BF16),
            vmem((3, OWN, half), BF16),
            vmem((3, OWN, half), BF16),
            vmem((3, OWN, half), BF16),
            DMA((2, 4)), DMA((2, 4)), DMA((3,)), DMA((3,)), DMA((3,)), DMA((3,)), DMA((3,)), DMA((3,)),
            DMA, DMA, DMA((3,)), DMA((3,)),
            DMA((2, 3)), DMA((2, 3)), DMA((3,)), DMA((2, 4, 2)), DMA((2, 4, 2)), DMA((8, 2)), DMA((8, 2)), DMA, DMA((2,)),
            DMA((2, 3)), DMA((2, 3)), DMA((2, 3)), DMA((2, 3)), DMA((2, 3)), DMA((2, 3)), DMA((2, 3)), DMA((2, 3)),
        ],
        compiler_params=pltpu.CompilerParams(collective_id=0, has_side_effects=True, vmem_limit_bytes=63 * 2**20),
        name="layer",
    )(
        query_a, key_a, value_a, query_b, key_b.T, value_b.T, gain_a, gain_b, jnp.asarray(rowtab), jnp.asarray(coltab),
        out_a, out_b, residual.reshape(NX * NC, OWN, D), norm_gain.reshape(1, D), gate_weight, up_weight,
        down_weight.reshape(2, 3, 128, 128),
    )


def solution(mesh):
    return jax.shard_map(
        on_device,
        mesh=mesh,
        in_specs=(
            P("sp", "tp"), P("sp", "tp"), P("sp", "tp"), P("sp", "tp"), P("sp", "tp"), P("sp", "tp"),
            P(), P(), P("tp", None), P("tp", None), P("sp", None), P(),
            P("sp", "tp"), P("sp", "tp"), P("tp", "sp"),
        ),
        out_specs=P(("sp", "tp"), None),
        check_vma=False,
    )
```

time: 146 us -> 125 us (0.86)
  Pallas kernels: 141 us -> 123 us
  other arithmetic: 2.15 us -> 0 us
  local copies, waits for them, and re-layouts: 3.36 us -> 1.62 us
    pallas_call x2 -> x1, Pallas kernels: 141 us -> 123 us  [on_device(): pl.pallas_call(layer_kernel, out_shape=jax.ShapeDtypeStruct((OWN, D), BF1...]
    concatenate x2 -> x0, other arithmetic: 2.15 us -> none  [the longest x1 1.42 us: on_device(): jnp.concatenate([gain_a, jnp.concatenate([gain_b, gain_b], axis=1)], axis=0)]
    unnamed x3 -> x1, local copies, waits for them, and re-layouts: 3.36 us -> 1.62 us
where the time goes in v2:
time: 125 us
  Pallas kernels  123 us (98%)
  local copies, waits for them, and re-layouts  1.62 us (1%)
    pallas_call x1, Pallas kernels, on_device(): pl.pallas_call(layer_kernel, out_shape=jax.ShapeDtypeStruct((OWN, D), BF1...  123 us

profile of v2, /device:TPU:1, one launch (start us, length us, event | category | flops | bytes accessed | tf_op | source)
XLA Modules:
  0.0 125.0 jit_solution(8145999585505511911)
XLA Ops:
  0.0 123.4 %layer.1 = bf16[24,4096]{1,0:T(8,128)(2,1)} custom-call(bf16[192,256]{1,0:T(8,128)(2,1)} %qa.1, bf16[192,128]{1,0:T(8,128)(2,1)} %ka.1, bf16[192,128]{1,0:T(8,128)(2,1)} %va.1, bf16[192,256]{1,0:T(8,128)(2,1)} %qb.1, bf16[64,192]{1,0:T(8,128)(2,1)} %bitcast.7, bf16[64,192]{1,0:T(8,128)(2,1)} %bitcast.8, f32[2,128]{1,0:T(2,128)} %gain_a.1, f32[2,64]{1,0:T(2,128)} %gain_b.1, ...), custom_call_target="tpu_custom_call" | custom-call | tf_op jit(solution)/shard_map/layer/pallas_call | solution.py:439
  123.4 1.6 %copy.19 = bf16[24,4096]{1,0:T(8,128)(2,1)} copy(bf16[24,4096]{1,0:T(8,128)(2,1)} %layer.1) | data formatting | bytes 393216

commit v3 on v2

v3 whole, which is shorter than its diff:
```python
import jax
import jax.numpy as jnp
import numpy as np
from jax import lax
from jax.experimental import pallas as pl
from jax.experimental.pallas import tpu as pltpu
from jax.sharding import PartitionSpec as P

NZ, NY, NX, NC = 8, 4, 4, 2
ROWS = 192
OWN = 24
HEAD_A, HEAD_B, GRID_W = 128, 64, 64
D = 4096
HID = 384
EPS = 1e-06
BASE = 10000.0
MESH = pl.DeviceIdType.MESH
F32, BF16 = jnp.float32, jnp.bfloat16


def turn_tables():
    rows, cols = [], []
    for head in (HEAD_A, HEAD_B):
        quarter = head // 4
        freq = np.float32(BASE) ** (-4.0 * np.arange(quarter, dtype=np.float32) / head).astype(np.float32)
        lane = np.arange(128)
        lane_freq = freq[lane % quarter]
        sign = np.where((lane // quarter) % 2 == 0, -1.0, 1.0).astype(np.float32)
        for positions, out in ((np.arange(96), rows), (np.arange(64), cols)):
            angle = (positions.astype(np.float32)[:, None] * lane_freq[None, :]).astype(np.float32)
            out.append(np.cos(angle).astype(np.float32))
            out.append((np.sin(angle) * sign).astype(np.float32))
    return np.stack(rows), np.stack(cols)


def place():
    sp, tp = lax.axis_index("sp"), lax.axis_index("tp")
    return sp // NY, sp % NY, tp // NC, tp % NC


def at(z, y, x, c):
    return (z * NY + y, x * NC + c)


def send(src, dst, send_sem, recv_sem, device):
    copy = pltpu.make_async_remote_copy(
        src_ref=src, dst_ref=dst, send_sem=send_sem, recv_sem=recv_sem, device_id=device, device_id_type=MESH
    )
    copy.start()
    return copy


def greet(devices):
    barrier = pltpu.get_barrier_semaphore()
    for device in devices:
        pl.semaphore_signal(barrier, inc=1, device_id=device, device_id_type=MESH)
    pl.semaphore_wait(barrier, len(devices))


HEADS = 6
LOG2E = 1.4426950408889634
SLOT = {0: 0, 1: 1, -1: 2, 2: 3, -2: 4, 3: 5, -3: 6, 4: 7}
EARLY = 5 * ROWS


def layer_kernel(
    qa, ka, va, qb, kb, vb, gain_a, gain_b, rowtab, coltab, outa_any, outb_any, resid, norm_gain, gate, up, down,
    out,
    kv, qs, qx, run_acc, late_acc, run_stat, part, parts_in, stat, stats_in, attn, outa, outb, proj, proj_in, sums, sums_in,
    own_resid, mixed, normed, tokens, wgu, wdn, acc, hidden, parts, r_in, r_add, f_in, f_sum, f_add,
    kv_send, kv_recv, q_send, q_recv, p_send, p_recv, s_send, s_recv, d_send, d_recv, x_send, x_recv,
    wa_send, wa_recv, wa_local, wz_send, wz_recv, wc_send, wc_recv, l_sem, o_sem,
    g_send, g_recv, h_send, h_recv, r_send, r_recv, f_send, f_recv,
):
    z, y, x, c = place()
    ys = [(y + d) % NY for d in range(NY)]
    xs = [(x + d) % NX for d in range(NX)]
    to_y = [at(z, ys[d], x, c) for d in range(NY)]
    to_x = [at(z, y, xs[d], c) for d in range(NX)]
    up_z, down_z = at((z + 1) % NZ, y, x, c), at((z + NZ - 1) % NZ, y, x, c)
    other = at(z, y, x, 1 - c)

    loads = [
        pltpu.make_async_copy(resid.at[x * NC + c], own_resid, l_sem),
        pltpu.make_async_copy(outa_any, outa, o_sem.at[0]),
        pltpu.make_async_copy(outb_any, outb, o_sem.at[1]),
    ]
    for copy in loads:
        copy.start()

    lane = lax.broadcasted_iota(jnp.int32, (ROWS, 128), 1)
    low = lane < 64

    def table(kind, half):
        sp = z * NY + y
        row = jnp.concatenate(
            [jnp.broadcast_to(rowtab[kind, pl.ds(sp * 3 + r, 1), :], (64, 128)) for r in range(3)], axis=0
        )
        col = jnp.concatenate([coltab[kind]] * 3, axis=0)
        return jnp.where(lane % (2 * half) < half, row, col)

    def turned(v, gain, cos, sin, head):
        quarter = head // 4
        v = v.astype(F32)
        sq = v * v
        if head == 128:
            mean = jnp.sum(sq, axis=-1, keepdims=True) * (1.0 / 128)
        else:
            first = jnp.sum(jnp.where(low, sq, 0.0), axis=-1, keepdims=True)
            second = jnp.sum(jnp.where(low, 0.0, sq), axis=-1, keepdims=True)
            mean = jnp.where(low, first, second) * (1.0 / 64)
        v = v * lax.rsqrt(mean + EPS) * gain
        even = (lane // quarter) % 2 == 0
        rolled = jnp.where(even, pltpu.roll(v, 128 - quarter, 1), pltpu.roll(v, quarter, 1))
        return v * cos + rolled * sin

    def twice(v):
        return jnp.concatenate([v, v], axis=-1)

    cos_a, sin_a = table(0, 64), table(1, 64)
    cos_b, sin_b = table(2, 32), table(3, 32)
    kv[0, :, 0:128] = turned(ka[...], gain_a[1:2, :], cos_a, sin_a, 128).astype(BF16)
    kv[0, :, 128:256] = va[...]
    kb_now = jnp.concatenate([kb[...].astype(F32), vb[...].astype(F32)], axis=0).T
    kv[0, :, 256:384] = jnp.where(low, turned(kb_now, twice(gain_b[1:2, :]), cos_b, sin_b, 64), kb_now).astype(BF16)

    for t in range(2):
        qs[0, t] = turned(qa[:, t * 128 : t * 128 + 128], gain_a[0:1, :], cos_a, sin_a, 128).astype(BF16)
    for t in range(2):
        qs[0, 2 + t] = turned(qb[:, t * 128 : t * 128 + 128], twice(gain_b[0:1, :]), cos_b, sin_b, 64).astype(BF16)
    greet(to_y[1:] + [at(z, ys[d], x, 1 - c) for d in range(4)] + to_x[1:] + [up_z, down_z])

    def kv_step(s, piece):
        copies = []
        for k, sign in ((0, -1), (1, 1)):
            if s == 4 and k != piece:
                continue
            rows = pl.ds(96 * piece, 96)
            copies.append(
                send(
                    kv.at[SLOT[sign * (s - 1)], rows], kv.at[SLOT[sign * s] if s < 4 else 7, rows],
                    kv_send.at[k, s - 1, piece], kv_recv.at[k, s - 1, piece], (up_z, down_z)[k],
                )
            )
        return copies

    def arrived(copies):
        for copy in copies:
            copy.wait_recv()

    kv_steps = {(1, p): kv_step(1, p) for p in range(2)}
    q_copies = {d: send(qs.at[0], qs.at[4 - d], q_send.at[d - 1], q_recv.at[d - 1], to_y[d]) for d in (1, 3, 2)}

    def down_cols(zz, yy, count):
        return wdn.at[:, :, pl.ds(pl.multiple_of((zz * NY + yy) * 128, 128), count * 128)]

    def first_pieces(h):
        return [
            (gate.at[:, pl.ds(h * HID, HID)], wgu.at[z, y, :, pl.ds(0, HID)]),
            (up.at[:, pl.ds(h * HID, HID)], wgu.at[z, y, :, pl.ds(HID, HID)]),
            (down.at[h], down_cols(z, y, 1)),
        ]

    def stays(h):
        return jnp.logical_and(2 * c + h == y, y // 2 == c)

    for h in range(2):

        @pl.when(stays(h))
        def _():
            for i, (src, dst) in enumerate(first_pieces(h)):
                pltpu.make_async_copy(src, dst, wa_local.at[i]).start()

        @pl.when(jnp.logical_not(stays(h)))
        def _():
            for i, (src, dst) in enumerate(first_pieces(h)):
                send(src, dst, wa_send.at[h, i], wa_recv.at[y % 2, i], at(z, 2 * c + h, x, y // 2))

    def w_refs(zz, p):
        return [wgu.at[zz, pl.ds(2 * c + p, 1)], down_cols(zz, 2 * c + p, 1)]

    def w_step(s, turn):
        copies = []
        for k, sign in ((0, -1), (1, 1)):
            for i, ref in enumerate(w_refs((z + NZ + sign * (s - 1)) % NZ, turn ^ k)):
                copies.append(
                    send(ref, ref, wz_send.at[k, s - 1, turn, i], wz_recv.at[k, s - 1, turn, i], (up_z, down_z)[k])
                )
        return copies

    across = []

    def w_across(offset, p):
        zz = (z + NZ + offset) % NZ
        for i, ref in enumerate(w_refs(zz, p)):
            across.append(send(ref, ref, wc_send.at[offset % NZ, p, i], wc_recv.at[offset % NZ, p, i], other))

    w_steps = {}

    def w_on(s, turn):
        arrived(w_steps[s, turn])
        if s < 3 or (s == 3 and turn == 0):
            w_steps[s + 1, turn] = w_step(s + 1, turn)
        if s < 4:
            w_across(-s, turn)
            w_across(s, 1 - turn)
        else:
            w_across(4, 0)
            w_across(4, 1)

    for s in (1, 2):
        for p in range(2):
            arrived(kv_steps[s, p])
            kv_steps[s + 1, p] = kv_step(s + 1, p)

    contract = (((1,), (1,)), ((), ()))

    def scores(yy, unit, slots, count):
        if unit == 0:
            q = qs[yy, 0:2].reshape(2 * ROWS, 128)
            k = kv[slots, :, 0:128].reshape(count, 128)
        else:
            q = qx[yy, 2 * unit - 2 : 2 * unit].reshape(2 * ROWS, 128)
            k = kv[slots, :, 256:384].reshape(count, 128)
        return lax.dot_general(q, k, contract, preferred_element_type=F32)

    def blend(unit, score, slots, count):
        scale = (HEAD_A if unit == 0 else HEAD_B) ** -0.5 * LOG2E
        v = kv[slots, :, 128:256] if unit == 0 else kv[slots, :, 256:384]
        top = jnp.max(score, axis=-1, keepdims=True)
        weight = jnp.exp2((score - top) * scale)
        total = jnp.sum(weight, axis=-1, keepdims=True)
        return top * scale, total, jnp.dot(weight.astype(BF16), v.reshape(count, 128), preferred_element_type=F32)

    def attend(blocks, slots, count, note, close):
        jobs = [(yy, unit) for yy in blocks for unit in range(3)]
        ahead = scores(*jobs[0], slots, count)
        for i, (yy, unit) in enumerate(jobs):
            score = ahead
            if i + 1 < len(jobs):
                ahead = scores(*jobs[i + 1], slots, count)
            note(yy, unit, *blend(unit, score, slots, count))
            if unit == 2:
                close(yy)

    state = {}

    def noted(yy, unit, top, total):
        tops, totals = state.get(yy, (jnp.zeros((ROWS, 128), F32), jnp.ones((ROWS, 128), F32)))
        for j in range(2):
            rows = slice(j * ROWS, j * ROWS + ROWS)
            tops = jnp.where(lane == 2 * unit + j, top[rows], tops)
            totals = jnp.where(lane == 2 * unit + j, total[rows], totals)
        state[yy] = (tops, totals)

    def spread(yy):
        for t in range(2):
            pair = qs[yy, 2 + t].astype(F32)
            qx[yy, 2 * t] = jnp.where(low, pair, 0.0).astype(BF16)
            qx[yy, 2 * t + 1] = jnp.where(low, pltpu.roll(pair, 64, 1), 0.0).astype(BF16)

    def early_note(yy, unit, top, total, blended):
        run_acc[yy, 2 * unit : 2 * unit + 2] = blended.reshape(2, ROWS, 128)
        noted(yy, unit, top, total)

    def early_close(yy):
        run_stat[yy, 0], run_stat[yy, 1] = state.pop(yy)

    def late_note(yy, unit, top, total, blended):
        late_acc[2 * unit : 2 * unit + 2] = blended.reshape(2, ROWS, 128)
        noted(yy, unit, top, total)

    def late_close(yy):
        tops, totals = state.pop(yy)
        best = jnp.maximum(run_stat[yy, 0], tops)
        share0, share1 = jnp.exp2(run_stat[yy, 0] - best), jnp.exp2(tops - best)
        all_total = share0 * run_stat[yy, 1] + share1 * totals
        inverse = 1.0 / all_total
        share0, share1 = share0 * inverse, share1 * inverse
        done = [
            share0[:, j : j + 1] * run_acc[yy, j] + share1[:, j : j + 1] * late_acc[j] for j in range(HEADS)
        ]
        stats = best + jnp.log2(all_total)
        part[yy, 0] = done[0].astype(BF16)
        part[yy, 1] = done[1].astype(BF16)
        for t in range(2):
            part[yy, 2 + t] = jnp.where(low, pltpu.roll(done[2 + 2 * t], 64, 1), done[3 + 2 * t]).astype(BF16)
        stat[yy] = jnp.concatenate([stats, stats[0:64]], axis=0).T[0:8, :]
        if yy:
            p_copies.extend(p_send_to(yy))

    def p_send_to(d):
        return [
            send(part.at[d], parts_in.at[d - 1], p_send.at[d - 1], p_recv.at[d - 1], to_y[d]),
            send(stat.at[d], stats_in.at[d - 1], s_send.at[d - 1], s_recv.at[d - 1], to_y[d]),
        ]

    arrived([q_copies[3], q_copies[1]])
    for yy in (0, 1, 3):
        spread(yy)
    attend((0, 1), slice(0, 5), EARLY, early_note, early_close)
    for p in range(2):
        arrived(kv_steps[3, p])
        kv_steps[4, p] = kv_step(4, p)
    for i in range(2):
        landing = [wgu.at[z, 2 * c + i, :, pl.ds(0, HID)], wgu.at[z, 2 * c + i, :, pl.ds(HID, HID)], down_cols(z, 2 * c + i, 1)]
        home = jnp.logical_and(y // 2 == c, y == 2 * c + i)

        @pl.when(home)
        def _():
            for j, ref in enumerate(landing):
                pltpu.make_async_copy(ref, ref, wa_local.at[j]).wait()

        @pl.when(jnp.logical_not(home))
        def _():
            for j, ref in enumerate(landing):
                pltpu.make_async_copy(ref, ref, wa_recv.at[i, j]).wait()

    for turn in range(2):
        w_steps[1, turn] = w_step(1, turn)
    w_across(0, 0)
    w_across(0, 1)
    arrived([q_copies[2]])
    spread(2)
    attend((3, 2), slice(0, 5), EARLY, early_note, early_close)
    arrived(kv_steps[4, 0] + kv_steps[4, 1])
    p_copies = []
    attend((2, 1, 3, 0), slice(5, 8), 3 * ROWS, late_note, late_close)
    w_on(1, 0)
    arrived(p_copies)

    def columns(block):
        return jnp.concatenate([block, jnp.zeros((120, 256), F32)], axis=0).T[0:ROWS, :]

    levels = [columns(stat[0])] + [columns(stats_in[d]) for d in range(3)]
    best = jnp.maximum(jnp.maximum(levels[0], levels[1]), jnp.maximum(levels[2], levels[3]))
    shares = [jnp.exp2(v - best) for v in levels]
    inverse = 1.0 / (shares[0] + shares[1] + shares[2] + shares[3])
    shares = [v * inverse for v in shares]
    for t in range(4):
        total = jnp.zeros((ROWS, 128), F32)
        for d in range(4):
            block = part[0, t] if d == 0 else parts_in[d - 1, t]
            if t < 2:
                share = shares[d][:, t : t + 1]
            else:
                share = jnp.where(low, shares[d][:, 2 * t - 2 : 2 * t - 1], shares[d][:, 2 * t - 1 : 2 * t])
            total = total + share * block.astype(F32)
        attn[:, t * 128 : t * 128 + 128] = total.astype(BF16)

    for copy in loads:
        copy.wait()
    half = D // 2
    halves = (pl.ds(0, half), pl.ds(half, half))

    d_copies = []
    for part_of in range(2):

        @pl.loop(part_of * 4, part_of * 4 + 4)
        def _(n):
            cols = pl.ds(pl.multiple_of(n * 512, 512), 512)
            now = jnp.dot(attn[:, 0:256], outa[:, cols], preferred_element_type=F32)
            now = now + jnp.dot(attn[:, 256:512], outb[:, cols], preferred_element_type=F32)
            proj[:, :, :, cols] = now.reshape(NX, NC, OWN, 512).astype(BF16)

        cols = halves[part_of]
        d_copies.append(
            send(proj.at[:, 1 - c, :, cols], proj_in.at[:, :, cols], d_send.at[part_of], d_recv.at[part_of], other)
        )
    x_copies = []
    for part_of in range(2):
        cols = halves[part_of]
        d_copies[part_of].wait_recv()
        for d in (2, 1, 3):
            sums[d - 1, :, cols] = (proj[xs[d], c, :, cols].astype(F32) + proj_in[xs[d], :, cols].astype(F32)).astype(BF16)
            x_copies.append(
                send(
                    sums.at[d - 1, :, cols], sums_in.at[d - 1, :, cols],
                    x_send.at[part_of, d - 1], x_recv.at[part_of, d - 1], to_x[d],
                )
            )
    mixed[...] = own_resid[...].astype(F32) + (proj[x, c].astype(F32) + proj_in[x].astype(F32))
    w_on(1, 1)
    w_on(2, 0)
    arrived(x_copies)
    total = mixed[...] + sums_in[0].astype(F32) + sums_in[1].astype(F32) + sums_in[2].astype(F32)
    mixed[...] = total
    mean = jnp.sum(total * total, axis=-1, keepdims=True) * (1.0 / D)
    normed[...] = (total * lax.rsqrt(mean + EPS) * norm_gain[...]).astype(BF16)
    tokens[0, 0] = normed[...]

    quart = half // 2

    def ring(h, first):
        return (to_x[1], to_x[3]) if (h == 0) == first else (to_y[1], to_y[3])

    def slot(h, e1, e2, lo, width):
        cols = pl.ds(h * half + lo, width)
        return tokens.at[e2, e1, :, cols] if h == 0 else tokens.at[e1, e2, :, cols]

    def hop(h, k, e1, second, on):
        lo, width = (k * quart, quart) if on else (0, half)
        step = -1 if k == 0 else 1
        if second:
            e2 = step % 4 if on else 0
            src, dst = slot(h, e1, e2, lo, width), slot(h, e1, (e2 + step) % 4, lo, width)
            sems = (h_send.at[h, e1, k, on], h_recv.at[h, e1, k, on])
        else:
            src, dst = slot(h, e1, 0, lo, width), slot(h, (e1 + step) % 4, 0, lo, width)
            sems = (g_send.at[h, k, on], g_recv.at[h, k, on])
        return send(src, dst, *sems, ring(h, not second)[k])

    both = [(h, k) for h in range(2) for k in range(2)]
    line = {(h, k): hop(h, k, 0, False, 0) for h, k in both}
    plane = {(h, 0, k): hop(h, k, 0, True, 0) for h, k in both}
    line_on, plane_on = {}, {}
    w_on(2, 1)
    for h, k in both:
        line[h, k].wait_recv()
        got = 3 if k == 0 else 1
        line_on[h, k] = hop(h, k, got, False, 1)
        for k2 in range(2):
            plane[h, got, k2] = hop(h, k2, got, True, 0)
    for h, k in both:
        plane[h, 0, k].wait_recv()
        plane_on[h, 0, k] = hop(h, k, 0, True, 1)
    for h in range(2):
        arrived([line_on[h, 0], line_on[h, 1]])
        for k in range(2):
            plane[h, 2, k] = hop(h, k, 2, True, 0)
    w_on(3, 0)
    for e1 in (3, 1):
        for h, k in both:
            plane[h, e1, k].wait_recv()
            plane_on[h, e1, k] = hop(h, k, e1, True, 1)
    for h, k in both:
        plane[h, 2, k].wait_recv()
        plane_on[h, 2, k] = hop(h, k, 2, True, 1)
    w_on(3, 1)
    arrived(plane_on.values())
    w_on(4, 0)
    arrived(across)

    count = NY * NX * OWN

    @pl.loop(0, 8)
    def _(n):
        cols = pl.ds(pl.multiple_of(n * 512, 512), 512)
        block = tokens[:, :, :, cols].astype(F32).reshape(count, 512).astype(BF16)
        now = jnp.dot(block, wgu[pl.ds(n, 1)].reshape(512, 2 * HID), preferred_element_type=F32)

        @pl.when(n == 0)
        def _():
            acc[...] = now

        @pl.when(n > 0)
        def _():
            acc[...] += now

    gated = acc[:, 0:HID]
    hidden[...] = (gated / (1.0 + jnp.exp(-gated)) * acc[:, HID : 2 * HID]).astype(BF16)

    @pl.loop(0, 8)
    def _(n):
        cols = pl.ds(pl.multiple_of(n * 512, 512), 512)
        now = jnp.dot(hidden[...], wdn[:, :, cols].reshape(HID, 512), preferred_element_type=F32)
        parts[:, :, :, cols] = now.reshape(NY, NX, OWN, 512).astype(BF16)

    def block(h, d1, d2, lo):
        cols = pl.ds(h * half + lo * quart, quart)
        return parts.at[d1, d2, :, cols] if h == 0 else parts.at[d2, d1, :, cols]

    def r_move(kind, h, d2, k, src):
        return send(src, r_in.at[kind, h, d2, k], r_send.at[kind, h, d2, k], r_recv.at[kind, h, d2, k], ring(h, False)[k])

    def f_move(kind, h, k, src):
        return send(src, f_in.at[kind, h, k], f_send.at[kind, h, k], f_recv.at[kind, h, k], ring(h, True)[k])

    order = (2, 1, 3, 0)
    moves = {(0, h, d2, k): r_move(0, h, d2, k, block(h, 2, d2, k)) for d2 in order for h, k in both}
    for d2 in order:
        for h, k in both:
            moves[1, h, d2, k] = r_move(1, h, d2, k, block(h, 1 + 2 * k, d2, 1 - k))
        for h, k in both:
            moves[0, h, d2, k].wait_recv()
            r_add[h, d2, k] = (block(h, 1 + 2 * k, d2, k)[...].astype(F32) + r_in[0, h, d2, k].astype(F32)).astype(BF16)
            moves[2, h, d2, k] = r_move(2, h, d2, k, r_add.at[h, d2, k])
    ends, totals = {}, {}

    def landed(h, d2):
        for k in range(2):
            arrived([moves[1, h, d2, k], moves[2, h, d2, k]])
        return [
            block(h, 0, d2, k)[...].astype(F32) + r_in[2, h, d2, k].astype(F32) + r_in[1, h, d2, 1 - k].astype(F32)
            for k in range(2)
        ]

    for d2 in order:
        for h in range(2):
            now = landed(h, d2)
            if d2 == 0:
                totals[h] = now
                continue
            for k in range(2):
                f_sum[h, d2, k] = now[k].astype(BF16)
            if d2 == 2:
                for k in range(2):
                    ends[0, h, k] = f_move(0, h, k, f_sum.at[h, 2, k])
            else:
                k = (d2 - 1) // 2
                ends[1, h, k] = f_move(1, h, k, f_sum.at[h, d2, 1 - k])
                ends[0, h, k].wait_recv()
                f_add[h, k] = (now[k] + f_in[0, h, k].astype(F32)).astype(BF16)
                ends[2, h, k] = f_move(2, h, k, f_add.at[h, k])
    for h in range(2):
        for k in range(2):
            arrived([ends[2, h, k], ends[1, h, 1 - k]])
            cols = slice(h * half + k * quart, h * half + k * quart + quart)
            total = totals[h][k] + f_in[2, h, k].astype(F32) + f_in[1, h, 1 - k].astype(F32)
            out[:, cols] = (mixed[:, cols] + 0.5 * total).astype(BF16)

    for copy in sum(kv_steps.values(), []) + list(q_copies.values()) + sum(w_steps.values(), []) + across + p_copies:
        copy.wait_send()
    for group in (line, line_on, plane, plane_on, moves, ends):
        for copy in group.values():
            copy.wait_send()
    for copy in d_copies + x_copies:
        copy.wait_send()
    for h in range(2):

        @pl.when(jnp.logical_not(stays(h)))
        def _():
            for i, (src, dst) in enumerate(first_pieces(h)):
                pltpu.make_async_copy(dst, dst, wa_send.at[h, i]).wait()


VM = pl.BlockSpec(memory_space=pltpu.VMEM)
ANY = pl.BlockSpec(memory_space=pl.ANY)
DMA = pltpu.SemaphoreType.DMA


def on_device(
    query_a, key_a, value_a, query_b, key_b, value_b, gain_a, gain_b, out_a, out_b, residual, norm_gain,
    gate_weight, up_weight, down_weight,
):
    rowtab, coltab = turn_tables()
    vmem = pltpu.VMEM
    return pl.pallas_call(
        layer_kernel,
        out_shape=jax.ShapeDtypeStruct((OWN, D), BF16),
        in_specs=[VM] * 10 + [ANY] * 3 + [VM] + [ANY] * 3,
        out_specs=VM,
        scratch_shapes=[
            vmem((NZ, ROWS, 384), BF16),
            vmem((NY, 4, ROWS, 128), BF16),
            vmem((NY, 4, ROWS, 128), BF16),
            vmem((NY, HEADS, ROWS, 128), F32),
            vmem((HEADS, ROWS, 128), F32),
            vmem((NY, 2, ROWS, 128), F32),
            vmem((NY, 4, ROWS, 128), BF16),
            vmem((3, 4, ROWS, 128), BF16),
            vmem((NY, 8, 256), F32),
            vmem((3, 8, 256), F32),
            vmem((ROWS, 512), BF16),
            vmem((256, D), BF16),
            vmem((256, D), BF16),
            vmem((NX, NC, OWN, D), BF16),
            vmem((NX, OWN, D), BF16),
            vmem((3, OWN, D), BF16),
            vmem((3, OWN, D), BF16),
            vmem((OWN, D), BF16),
            vmem((OWN, D), F32),
            vmem((OWN, D), BF16),
            vmem((NY, NX, OWN, D), BF16),
            vmem((NZ, NY, 128, 2 * HID), BF16),
            vmem((3, 128, D), BF16),
            vmem((NY * NX * OWN, 2 * HID), F32),
            vmem((NY * NX * OWN, HID), BF16),
            vmem((NY, NX, OWN, D), BF16),
            vmem((3, 2, 4, 2, OWN, D // 4), BF16),
            vmem((2, 4, 2, OWN, D // 4), BF16),
            vmem((3, 2, 2, OWN, D // 4), BF16),
            vmem((2, 4, 2, OWN, D // 4), BF16),
            vmem((2, 2, OWN, D // 4), BF16),
            DMA((2, 4, 2)), DMA((2, 4, 2)), DMA((3,)), DMA((3,)), DMA((3,)), DMA((3,)), DMA((3,)), DMA((3,)),
            DMA((2,)), DMA((2,)), DMA((2, 3)), DMA((2, 3)),
            DMA((2, 3)), DMA((2, 3)), DMA((3,)), DMA((2, 4, 2, 2)), DMA((2, 4, 2, 2)), DMA((8, 2, 2)), DMA((8, 2, 2)),
            DMA, DMA((2,)),
            DMA((2, 2, 2)), DMA((2, 2, 2)), DMA((2, 4, 2, 2)), DMA((2, 4, 2, 2)),
            DMA((3, 2, 4, 2)), DMA((3, 2, 4, 2)), DMA((3, 2, 2)), DMA((3, 2, 2)),
        ],
        compiler_params=pltpu.CompilerParams(collective_id=0, has_side_effects=True, vmem_limit_bytes=63 * 2**20),
        name="layer",
    )(
        query_a, key_a, value_a, query_b, key_b.T, value_b.T, gain_a, gain_b, jnp.asarray(rowtab), jnp.asarray(coltab),
        out_a, out_b, residual.reshape(NX * NC, OWN, D), norm_gain.reshape(1, D), gate_weight, up_weight,
        down_weight.reshape(2, 3, 128, 128),
    )


def solution(mesh):
    return jax.shard_map(
        on_device,
        mesh=mesh,
        in_specs=(
            P("sp", "tp"), P("sp", "tp"), P("sp", "tp"), P("sp", "tp"), P("sp", "tp"), P("sp", "tp"),
            P(), P(), P("tp", None), P("tp", None), P("sp", None), P(),
            P("sp", "tp"), P("sp", "tp"), P("tp", "sp"),
        ),
        out_specs=P(("sp", "tp"), None),
        check_vma=False,
    )
```

time: 125 us -> 114 us (0.912)
  Pallas kernels: 123 us -> 113 us
    pallas_call x1, Pallas kernels: 123 us -> 113 us  [on_device(): pl.pallas_call(layer_kernel, out_shape=jax.ShapeDtypeStruct((OWN, D), BF1...]
where the time goes in v3:
time: 114 us
  Pallas kernels  113 us (99%)
  local copies, waits for them, and re-layouts  1.62 us (1%)
    pallas_call x1, Pallas kernels, on_device(): pl.pallas_call(layer_kernel, out_shape=jax.ShapeDtypeStruct((OWN, D), BF1...  113 us

profile of v3, /device:TPU:1, one launch (start us, length us, event | category | flops | bytes accessed | tf_op | source)
XLA Modules:
  0.0 114.3 jit_solution(1096137992830675076)
XLA Ops:
  0.0 112.6 %layer.1 = bf16[24,4096]{1,0:T(8,128)(2,1)} custom-call(bf16[192,256]{1,0:T(8,128)(2,1)} %qa.1, bf16[192,128]{1,0:T(8,128)(2,1)} %ka.1, bf16[192,128]{1,0:T(8,128)(2,1)} %va.1, bf16[192,256]{1,0:T(8,128)(2,1)} %qb.1, bf16[64,192]{1,0:T(8,128)(2,1)} %bitcast.7, bf16[64,192]{1,0:T(8,128)(2,1)} %bitcast.8, f32[2,128]{1,0:T(2,128)} %gain_a.1, f32[2,64]{1,0:T(2,128)} %gain_b.1, ...), custom_call_target="tpu_custom_call" | custom-call | tf_op jit(solution)/shard_map/layer/pallas_call | solution.py:548
  112.6 1.6 %copy.19 = bf16[24,4096]{1,0:T(8,128)(2,1)} copy(bf16[24,4096]{1,0:T(8,128)(2,1)} %layer.1) | data formatting | bytes 393216

commit v4 on v3

--- a/solution.py
+++ b/solution.py
@@ -50,6 +50,10 @@
     return copy
 
 
+def settle(ref, sem):
+    pltpu.make_async_copy(ref, ref, sem).wait()
+
+
 def greet(devices):
     barrier = pltpu.get_barrier_semaphore()
     for device in devices:
@@ -67,10 +71,10 @@
     qa, ka, va, qb, kb, vb, gain_a, gain_b, rowtab, coltab, outa_any, outb_any, resid, norm_gain, gate, up, down,
     out,
     kv, qs, qx, run_acc, late_acc, run_stat, part, parts_in, stat, stats_in, attn, outa, outb, proj, proj_in, sums, sums_in,
-    own_resid, mixed, normed, tokens, wgu, wdn, acc, hidden, parts, r_in, r_add, f_in, f_sum, f_add,
+    own_resid, mixed, normed, tokens, lhs, wgu, wdn, acc, hidden, parts, r_in, r_add, f_in, f_sum, f_add,
     kv_send, kv_recv, q_send, q_recv, p_send, p_recv, s_send, s_recv, d_send, d_recv, x_send, x_recv,
     wa_send, wa_recv, wa_local, wz_send, wz_recv, wc_send, wc_recv, l_sem, o_sem,
-    g_send, g_recv, h_send, h_recv, r_send, r_recv, f_send, f_recv,
+    g_send, g_recv, g_on_recv, h_send, h_recv, h_on_recv, r_send, r_recv, f_send, f_recv, f_on_recv,
 ):
     z, y, x, c = place()
     ys = [(y + d) % NY for d in range(NY)]
@@ -139,7 +143,7 @@
             copies.append(
                 send(
                     kv.at[SLOT[sign * (s - 1)], rows], kv.at[SLOT[sign * s] if s < 4 else 7, rows],
-                    kv_send.at[k, s - 1, piece], kv_recv.at[k, s - 1, piece], (up_z, down_z)[k],
+                    kv_send, kv_recv.at[s - 1, piece if s < 4 else 0], (up_z, down_z)[k],
                 )
             )
         return copies
@@ -148,17 +152,18 @@
         for copy in copies:
             copy.wait_recv()
 
-    kv_steps = {(1, p): kv_step(1, p) for p in range(2)}
-    q_copies = {d: send(qs.at[0], qs.at[4 - d], q_send.at[d - 1], q_recv.at[d - 1], to_y[d]) for d in (1, 3, 2)}
-
-    def down_cols(zz, yy, count):
-        return wdn.at[:, :, pl.ds(pl.multiple_of((zz * NY + yy) * 128, 128), count * 128)]
+    for p in range(2):
+        kv_step(1, p)
+    def q_copy(d):
+        return send(qs.at[0], qs.at[4 - d], q_send, q_recv.at[d - 1], to_y[d])
+
+    q_copies = {d: q_copy(d) for d in (1, 3, 2)}
 
     def first_pieces(h):
         return [
-            (gate.at[:, pl.ds(h * HID, HID)], wgu.at[z, y, :, pl.ds(0, HID)]),
-            (up.at[:, pl.ds(h * HID, HID)], wgu.at[z, y, :, pl.ds(HID, HID)]),
-            (down.at[h], down_cols(z, y, 1)),
+            (gate.at[:, pl.ds(h * HID, HID)], wgu.at[0, y, :, pl.ds(0, HID)]),
+            (up.at[:, pl.ds(h * HID, HID)], wgu.at[0, y, :, pl.ds(HID, HID)]),
+            (down.at[h], wdn.at[0, y]),
         ]
 
     def stays(h):
@@ -168,50 +173,45 @@
 
         @pl.when(stays(h))
         def _():
-            for i, (src, dst) in enumerate(first_pieces(h)):
-                pltpu.make_async_copy(src, dst, wa_local.at[i]).start()
+            for src, dst in first_pieces(h):
+                pltpu.make_async_copy(src, dst, wa_local).start()
 
         @pl.when(jnp.logical_not(stays(h)))
         def _():
-            for i, (src, dst) in enumerate(first_pieces(h)):
-                send(src, dst, wa_send.at[h, i], wa_recv.at[y % 2, i], at(z, 2 * c + h, x, y // 2))
-
-    def w_refs(zz, p):
-        return [wgu.at[zz, pl.ds(2 * c + p, 1)], down_cols(zz, 2 * c + p, 1)]
-
-    def w_step(s, turn):
-        copies = []
-        for k, sign in ((0, -1), (1, 1)):
-            for i, ref in enumerate(w_refs((z + NZ + sign * (s - 1)) % NZ, turn ^ k)):
-                copies.append(
-                    send(ref, ref, wz_send.at[k, s - 1, turn, i], wz_recv.at[k, s - 1, turn, i], (up_z, down_z)[k])
-                )
-        return copies
-
-    across = []
-
-    def w_across(offset, p):
-        zz = (z + NZ + offset) % NZ
-        for i, ref in enumerate(w_refs(zz, p)):
-            across.append(send(ref, ref, wc_send.at[offset % NZ, p, i], wc_recv.at[offset % NZ, p, i], other))
-
-    w_steps = {}
-
-    def w_on(s, turn):
-        arrived(w_steps[s, turn])
+            for src, dst in first_pieces(h):
+                send(src, dst, wa_send.at[h], wa_recv.at[y % 2], at(z, 2 * c + h, x, y // 2))
+
+    def w_ref(kind, offset, p):
+        return (wgu, wdn)[kind].at[SLOT[offset], 2 * c + p]
+
+    def w_step(kind, s, turn):
+        return [
+            send(
+                w_ref(kind, sign * (s - 1), turn ^ k), w_ref(kind, sign * s if s < 4 else 4, turn ^ k),
+                wz_send.at[kind], wz_recv.at[kind, s - 1, turn], (up_z, down_z)[k],
+            )
+            for k, sign in ((0, -1), (1, 1))
+        ]
+
+    def w_across(kind, offset, p):
+        ref = w_ref(kind, offset, p)
+        send(ref, ref, wc_send.at[kind], wc_recv.at[kind + (kind == 1 and offset == 4)], other)
+
+    def w_on(kind, s, turn):
+        settle((wgu, wdn)[kind].at[0, pl.ds(0, 2)], wz_recv.at[kind, s - 1, turn])
         if s < 3 or (s == 3 and turn == 0):
-            w_steps[s + 1, turn] = w_step(s + 1, turn)
+            w_step(kind, s + 1, turn)
         if s < 4:
-            w_across(-s, turn)
-            w_across(s, 1 - turn)
+            w_across(kind, -s, turn)
+            w_across(kind, s, 1 - turn)
         else:
-            w_across(4, 0)
-            w_across(4, 1)
+            w_across(kind, 4, 0)
+            w_across(kind, 4, 1)
 
     for s in (1, 2):
         for p in range(2):
-            arrived(kv_steps[s, p])
-            kv_steps[s + 1, p] = kv_step(s + 1, p)
+            settle(kv.at[0], kv_recv.at[s - 1, p])
+            kv_step(s + 1, p)
 
     contract = (((1,), (1,)), ((), ()))
 
@@ -269,65 +269,69 @@
     def late_note(yy, unit, top, total, blended):
         late_acc[2 * unit : 2 * unit + 2] = blended.reshape(2, ROWS, 128)
         noted(yy, unit, top, total)
-
-    def late_close(yy):
-        tops, totals = state.pop(yy)
+        if unit == 0:
+            merged(yy, (0, 1))
+
+    def merged(yy, heads):
+        tops, totals = state[yy]
         best = jnp.maximum(run_stat[yy, 0], tops)
         share0, share1 = jnp.exp2(run_stat[yy, 0] - best), jnp.exp2(tops - best)
         all_total = share0 * run_stat[yy, 1] + share1 * totals
         inverse = 1.0 / all_total
         share0, share1 = share0 * inverse, share1 * inverse
-        done = [
-            share0[:, j : j + 1] * run_acc[yy, j] + share1[:, j : j + 1] * late_acc[j] for j in range(HEADS)
-        ]
-        stats = best + jnp.log2(all_total)
-        part[yy, 0] = done[0].astype(BF16)
-        part[yy, 1] = done[1].astype(BF16)
-        for t in range(2):
-            part[yy, 2 + t] = jnp.where(low, pltpu.roll(done[2 + 2 * t], 64, 1), done[3 + 2 * t]).astype(BF16)
+        done = [share0[:, j : j + 1] * run_acc[yy, j] + share1[:, j : j + 1] * late_acc[j] for j in heads]
+        if heads == (0, 1):
+            part[yy, 0] = done[0].astype(BF16)
+            part[yy, 1] = done[1].astype(BF16)
+        else:
+            for t in range(2):
+                part[yy, 2 + t] = jnp.where(low, pltpu.roll(done[2 * t], 64, 1), done[2 * t + 1]).astype(BF16)
+        if yy:
+            two = pl.ds(0 if heads == (0, 1) else 2, 2)
+            send(part.at[yy, two], parts_in.at[yy - 1, two], p_send, p_recv, to_y[yy])
+        return best + jnp.log2(all_total)
+
+    def late_close(yy):
+        stats = merged(yy, (2, 3, 4, 5))
+        state.pop(yy)
         stat[yy] = jnp.concatenate([stats, stats[0:64]], axis=0).T[0:8, :]
         if yy:
-            p_copies.extend(p_send_to(yy))
-
-    def p_send_to(d):
-        return [
-            send(part.at[d], parts_in.at[d - 1], p_send.at[d - 1], p_recv.at[d - 1], to_y[d]),
-            send(stat.at[d], stats_in.at[d - 1], s_send.at[d - 1], s_recv.at[d - 1], to_y[d]),
-        ]
+            send(stat.at[yy], stats_in.at[yy - 1], s_send, s_recv, to_y[yy])
 
     arrived([q_copies[3], q_copies[1]])
     for yy in (0, 1, 3):
         spread(yy)
     attend((0, 1), slice(0, 5), EARLY, early_note, early_close)
+    attend((3,), slice(0, 5), EARLY, early_note, early_close)
     for p in range(2):
-        arrived(kv_steps[3, p])
-        kv_steps[4, p] = kv_step(4, p)
+        settle(kv.at[0], kv_recv.at[2, p])
+        kv_step(4, p)
+    arrived([q_copies[2]])
+    spread(2)
+    attend((2,), slice(0, 5), EARLY, early_note, early_close)
+    first_size = wdn.at[0, pl.ds(0, 3)]
     for i in range(2):
-        landing = [wgu.at[z, 2 * c + i, :, pl.ds(0, HID)], wgu.at[z, 2 * c + i, :, pl.ds(HID, HID)], down_cols(z, 2 * c + i, 1)]
         home = jnp.logical_and(y // 2 == c, y == 2 * c + i)
 
         @pl.when(home)
         def _():
-            for j, ref in enumerate(landing):
-                pltpu.make_async_copy(ref, ref, wa_local.at[j]).wait()
+            settle(first_size, wa_local)
 
         @pl.when(jnp.logical_not(home))
         def _():
-            for j, ref in enumerate(landing):
-                pltpu.make_async_copy(ref, ref, wa_recv.at[i, j]).wait()
-
-    for turn in range(2):
-        w_steps[1, turn] = w_step(1, turn)
-    w_across(0, 0)
-    w_across(0, 1)
-    arrived([q_copies[2]])
-    spread(2)
-    attend((3, 2), slice(0, 5), EARLY, early_note, early_close)
-    arrived(kv_steps[4, 0] + kv_steps[4, 1])
-    p_copies = []
+            settle(first_size, wa_recv.at[i])
+
+    for kind in range(2):
+        for turn in range(2):
+            w_step(kind, 1, turn)
+    for kind in range(2):
+        w_across(kind, 0, 0)
+        w_across(kind, 0, 1)
+    settle(kv.at[0], kv_recv.at[3, 0])
     attend((2, 1, 3, 0), slice(5, 8), 3 * ROWS, late_note, late_close)
-    w_on(1, 0)
-    arrived(p_copies)
+    w_on(0, 1, 0)
+    settle(parts_in, p_recv)
+    settle(stats_in, s_recv)
 
     def columns(block):
         return jnp.concatenate([block, jnp.zeros((120, 256), F32)], axis=0).T[0:ROWS, :]
@@ -351,38 +355,31 @@
     for copy in loads:
         copy.wait()
     half = D // 2
-    halves = (pl.ds(0, half), pl.ds(half, half))
-
-    d_copies = []
-    for part_of in range(2):
-
-        @pl.loop(part_of * 4, part_of * 4 + 4)
-        def _(n):
-            cols = pl.ds(pl.multiple_of(n * 512, 512), 512)
-            now = jnp.dot(attn[:, 0:256], outa[:, cols], preferred_element_type=F32)
-            now = now + jnp.dot(attn[:, 256:512], outb[:, cols], preferred_element_type=F32)
-            proj[:, :, :, cols] = now.reshape(NX, NC, OWN, 512).astype(BF16)
-
-        cols = halves[part_of]
-        d_copies.append(
-            send(proj.at[:, 1 - c, :, cols], proj_in.at[:, :, cols], d_send.at[part_of], d_recv.at[part_of], other)
-        )
-    x_copies = []
-    for part_of in range(2):
-        cols = halves[part_of]
-        d_copies[part_of].wait_recv()
+
+    quarters = [pl.ds(i * (D // 4), D // 4) for i in range(4)]
+
+    def summed_on(i):
+        cols = quarters[i]
+        settle(proj_in.at[:, :, cols], d_recv.at[i])
         for d in (2, 1, 3):
             sums[d - 1, :, cols] = (proj[xs[d], c, :, cols].astype(F32) + proj_in[xs[d], :, cols].astype(F32)).astype(BF16)
-            x_copies.append(
-                send(
-                    sums.at[d - 1, :, cols], sums_in.at[d - 1, :, cols],
-                    x_send.at[part_of, d - 1], x_recv.at[part_of, d - 1], to_x[d],
-                )
-            )
+            send(sums.at[d - 1, :, cols], sums_in.at[d - 1, :, cols], x_send, x_recv, to_x[d])
+
+    for i, cols in enumerate(quarters):
+        now = jnp.dot(attn[:, 0:256], outa[:, cols], preferred_element_type=F32)
+        now = now + jnp.dot(attn[:, 256:512], outb[:, cols], preferred_element_type=F32)
+        proj[:, :, :, cols] = now.reshape(NX, NC, OWN, D // 4).astype(BF16)
+        send(proj.at[:, 1 - c, :, cols], proj_in.at[:, :, cols], d_send, d_recv.at[i], other)
+        if i > 1:
+            summed_on(i - 2)
+    summed_on(2)
+    summed_on(3)
     mixed[...] = own_resid[...].astype(F32) + (proj[x, c].astype(F32) + proj_in[x].astype(F32))
-    w_on(1, 1)
-    w_on(2, 0)
-    arrived(x_copies)
+    w_on(0, 1, 1)
+    w_on(1, 1, 0)
+    w_on(1, 1, 1)
+    w_on(0, 2, 0)
+    settle(sums_in, x_recv)
     total = mixed[...] + sums_in[0].astype(F32) + sums_in[1].astype(F32) + sums_in[2].astype(F32)
     mixed[...] = total
     mean = jnp.sum(total * total, axis=-1, keepdims=True) * (1.0 / D)
@@ -404,98 +401,107 @@
         if second:
             e2 = step % 4 if on else 0
             src, dst = slot(h, e1, e2, lo, width), slot(h, e1, (e2 + step) % 4, lo, width)
-            sems = (h_send.at[h, e1, k, on], h_recv.at[h, e1, k, on])
+            sems = (h_send, h_on_recv if on else h_recv.at[h, e1, k])
         else:
             src, dst = slot(h, e1, 0, lo, width), slot(h, (e1 + step) % 4, 0, lo, width)
-            sems = (g_send.at[h, k, on], g_recv.at[h, k, on])
+            sems = (g_send, g_on_recv if on else g_recv.at[h, k])
         return send(src, dst, *sems, ring(h, not second)[k])
 
     both = [(h, k) for h in range(2) for k in range(2)]
     line = {(h, k): hop(h, k, 0, False, 0) for h, k in both}
     plane = {(h, 0, k): hop(h, k, 0, True, 0) for h, k in both}
-    line_on, plane_on = {}, {}
-    w_on(2, 1)
+    w_on(0, 2, 1)
     for h, k in both:
         line[h, k].wait_recv()
         got = 3 if k == 0 else 1
-        line_on[h, k] = hop(h, k, got, False, 1)
+        hop(h, k, got, False, 1)
         for k2 in range(2):
             plane[h, got, k2] = hop(h, k2, got, True, 0)
     for h, k in both:
         plane[h, 0, k].wait_recv()
-        plane_on[h, 0, k] = hop(h, k, 0, True, 1)
-    for h in range(2):
-        arrived([line_on[h, 0], line_on[h, 1]])
-        for k in range(2):
-            plane[h, 2, k] = hop(h, k, 2, True, 0)
-    w_on(3, 0)
+        hop(h, k, 0, True, 1)
+    w_on(1, 2, 0)
+    w_on(1, 2, 1)
+    w_on(0, 3, 0)
+    settle(tokens.at[0, 0], g_on_recv)
+    for h, k in both:
+        plane[h, 2, k] = hop(h, k, 2, True, 0)
+    w_on(0, 3, 1)
     for e1 in (3, 1):
         for h, k in both:
             plane[h, e1, k].wait_recv()
-            plane_on[h, e1, k] = hop(h, k, e1, True, 1)
+            hop(h, k, e1, True, 1)
+    w_on(1, 3, 0)
     for h, k in both:
         plane[h, 2, k].wait_recv()
-        plane_on[h, 2, k] = hop(h, k, 2, True, 1)
-    w_on(3, 1)
-    arrived(plane_on.values())
-    w_on(4, 0)
-    arrived(across)
-
+        hop(h, k, 2, True, 1)
+    w_on(1, 3, 1)
+    w_on(0, 4, 0)
+    settle(tokens.at[0], h_on_recv)
     count = NY * NX * OWN
 
-    @pl.loop(0, 8)
+    def cols_of(n):
+        offset = ((n + 1) // 2) * (2 * (n % 2) - 1)
+        return pl.ds(pl.multiple_of(((z + NZ + offset) % NZ) * 512, 512), 512)
+
+    @pl.loop(0, NZ)
     def _(n):
-        cols = pl.ds(pl.multiple_of(n * 512, 512), 512)
-        block = tokens[:, :, :, cols].astype(F32).reshape(count, 512).astype(BF16)
-        now = jnp.dot(block, wgu[pl.ds(n, 1)].reshape(512, 2 * HID), preferred_element_type=F32)
-
-        @pl.when(n == 0)
-        def _():
-            acc[...] = now
-
-        @pl.when(n > 0)
-        def _():
-            acc[...] += now
+        lined = tokens[:, :, :, cols_of(n)].astype(F32).reshape(count, 512).astype(BF16)
+        lhs[:, pl.ds(pl.multiple_of(n * 512, 512), 512)] = lined
+
+    w_on(1, 4, 0)
+    settle(wgu.at[:, pl.ds(0, 2)], wc_recv.at[0])
+
+    @pl.loop(0, 3)
+    def _(n):
+        cols = pl.ds(pl.multiple_of(n * 256, 256), 256)
+        acc[:, cols] = jnp.dot(lhs[...], wgu[:, :, :, cols].reshape(D, 256), preferred_element_type=F32)
 
     gated = acc[:, 0:HID]
     hidden[...] = (gated / (1.0 + jnp.exp(-gated)) * acc[:, HID : 2 * HID]).astype(BF16)
 
-    @pl.loop(0, 8)
-    def _(n):
-        cols = pl.ds(pl.multiple_of(n * 512, 512), 512)
-        now = jnp.dot(hidden[...], wdn[:, :, cols].reshape(HID, 512), preferred_element_type=F32)
-        parts[:, :, :, cols] = now.reshape(NY, NX, OWN, 512).astype(BF16)
+    def lowered(n):
+        now = jnp.dot(
+            hidden[...], jnp.concatenate([wdn[n, yy] for yy in range(NY)], axis=1), preferred_element_type=F32
+        )
+        parts[:, :, :, cols_of(n)] = now.reshape(NY, NX, OWN, 512).astype(BF16)
+
+    settle(wdn.at[pl.ds(0, NZ - 1), pl.ds(0, 2)], wc_recv.at[1])
+    pl.loop(0, NZ - 1)(lowered)
+    settle(wdn.at[0, pl.ds(0, 2)], wc_recv.at[2])
+    lowered(NZ - 1)
 
     def block(h, d1, d2, lo):
         cols = pl.ds(h * half + lo * quart, quart)
         return parts.at[d1, d2, :, cols] if h == 0 else parts.at[d2, d1, :, cols]
 
     def r_move(kind, h, d2, k, src):
-        return send(src, r_in.at[kind, h, d2, k], r_send.at[kind, h, d2, k], r_recv.at[kind, h, d2, k], ring(h, False)[k])
+        send(src, r_in.at[kind, h, d2, k], r_send, r_recv.at[min(kind, 1), d2], ring(h, False)[k])
 
     def f_move(kind, h, k, src):
-        return send(src, f_in.at[kind, h, k], f_send.at[kind, h, k], f_recv.at[kind, h, k], ring(h, True)[k])
+        send(src, f_in.at[kind, h, k], f_send, f_on_recv if kind else f_recv.at[h, k], ring(h, True)[k])
 
     order = (2, 1, 3, 0)
-    moves = {(0, h, d2, k): r_move(0, h, d2, k, block(h, 2, d2, k)) for d2 in order for h, k in both}
     for d2 in order:
         for h, k in both:
-            moves[1, h, d2, k] = r_move(1, h, d2, k, block(h, 1 + 2 * k, d2, 1 - k))
+            r_move(0, h, d2, k, block(h, 2, d2, k))
+    for d2 in order:
         for h, k in both:
-            moves[0, h, d2, k].wait_recv()
+            r_move(1, h, d2, k, block(h, 1 + 2 * k, d2, 1 - k))
+        settle(r_in.at[0, 0, pl.ds(0, 2)], r_recv.at[0, d2])
+        for h, k in both:
             r_add[h, d2, k] = (block(h, 1 + 2 * k, d2, k)[...].astype(F32) + r_in[0, h, d2, k].astype(F32)).astype(BF16)
-            moves[2, h, d2, k] = r_move(2, h, d2, k, r_add.at[h, d2, k])
-    ends, totals = {}, {}
+            r_move(2, h, d2, k, r_add.at[h, d2, k])
+    totals = {}
 
     def landed(h, d2):
-        for k in range(2):
-            arrived([moves[1, h, d2, k], moves[2, h, d2, k]])
         return [
             block(h, 0, d2, k)[...].astype(F32) + r_in[2, h, d2, k].astype(F32) + r_in[1, h, d2, 1 - k].astype(F32)
             for k in range(2)
         ]
 
     for d2 in order:
+        settle(r_in.at[0, 0], r_recv.at[1, d2])
         for h in range(2):
             now = landed(h, d2)
             if d2 == 0:
@@ -505,33 +511,34 @@
                 f_sum[h, d2, k] = now[k].astype(BF16)
             if d2 == 2:
                 for k in range(2):
-                    ends[0, h, k] = f_move(0, h, k, f_sum.at[h, 2, k])
+                    f_move(0, h, k, f_sum.at[h, 2, k])
             else:
                 k = (d2 - 1) // 2
-                ends[1, h, k] = f_move(1, h, k, f_sum.at[h, d2, 1 - k])
-                ends[0, h, k].wait_recv()
+                f_move(1, h, k, f_sum.at[h, d2, 1 - k])
+                settle(f_in.at[0, 0, 0], f_recv.at[h, k])
                 f_add[h, k] = (now[k] + f_in[0, h, k].astype(F32)).astype(BF16)
-                ends[2, h, k] = f_move(2, h, k, f_add.at[h, k])
+                f_move(2, h, k, f_add.at[h, k])
+    settle(f_in.at[pl.ds(1, 2)], f_on_recv)
     for h in range(2):
         for k in range(2):
-            arrived([ends[2, h, k], ends[1, h, 1 - k]])
             cols = slice(h * half + k * quart, h * half + k * quart + quart)
             total = totals[h][k] + f_in[2, h, k].astype(F32) + f_in[1, h, 1 - k].astype(F32)
             out[:, cols] = (mixed[:, cols] + 0.5 * total).astype(BF16)
 
-    for copy in sum(kv_steps.values(), []) + list(q_copies.values()) + sum(w_steps.values(), []) + across + p_copies:
-        copy.wait_send()
-    for group in (line, line_on, plane, plane_on, moves, ends):
-        for copy in group.values():
-            copy.wait_send()
-    for copy in d_copies + x_copies:
-        copy.wait_send()
+    three = pl.ds(0, 3)
+    for ref, sem in (
+        (kv.at[pl.ds(0, 7)], kv_send), (qs.at[three], q_send), (parts_in, p_send), (stats_in, s_send),
+        (proj_in, d_send), (sums_in, x_send), (tokens.at[0, three], g_send), (tokens.at[three], h_send),
+        (r_in, r_send), (f_in, f_send),
+        (wgu.at[pl.ds(0, 7), pl.ds(0, 2)], wz_send.at[0]), (wdn.at[pl.ds(0, 7), pl.ds(0, 2)], wz_send.at[1]),
+        (wgu.at[:, pl.ds(0, 2)], wc_send.at[0]), (wdn.at[:, pl.ds(0, 2)], wc_send.at[1]),
+    ):
+        settle(ref, sem)
     for h in range(2):
 
         @pl.when(jnp.logical_not(stays(h)))
         def _():
-            for i, (src, dst) in enumerate(first_pieces(h)):
-                pltpu.make_async_copy(dst, dst, wa_send.at[h, i]).wait()
+            settle(first_size, wa_send.at[h])
 
 
 VM = pl.BlockSpec(memory_space=pltpu.VMEM)
@@ -572,8 +579,9 @@
             vmem((OWN, D), F32),
             vmem((OWN, D), BF16),
             vmem((NY, NX, OWN, D), BF16),
+            vmem((NY * NX * OWN, D), BF16),
             vmem((NZ, NY, 128, 2 * HID), BF16),
-            vmem((3, 128, D), BF16),
+            vmem((NZ, NY, HID, 128), BF16),
             vmem((NY * NX * OWN, 2 * HID), F32),
             vmem((NY * NX * OWN, HID), BF16),
             vmem((NY, NX, OWN, D), BF16),
@@ -582,19 +590,17 @@
             vmem((3, 2, 2, OWN, D // 4), BF16),
             vmem((2, 4, 2, OWN, D // 4), BF16),
             vmem((2, 2, OWN, D // 4), BF16),
-            DMA((2, 4, 2)), DMA((2, 4, 2)), DMA((3,)), DMA((3,)), DMA((3,)), DMA((3,)), DMA((3,)), DMA((3,)),
-            DMA((2,)), DMA((2,)), DMA((2, 3)), DMA((2, 3)),
-            DMA((2, 3)), DMA((2, 3)), DMA((3,)), DMA((2, 4, 2, 2)), DMA((2, 4, 2, 2)), DMA((8, 2, 2)), DMA((8, 2, 2)),
-            DMA, DMA((2,)),
-            DMA((2, 2, 2)), DMA((2, 2, 2)), DMA((2, 4, 2, 2)), DMA((2, 4, 2, 2)),
-            DMA((3, 2, 4, 2)), DMA((3, 2, 4, 2)), DMA((3, 2, 2)), DMA((3, 2, 2)),
+            DMA, DMA((4, 2)), DMA, DMA((3,)), DMA, DMA, DMA, DMA,
+            DMA, DMA((4,)), DMA, DMA,
+            DMA((2,)), DMA((2,)), DMA, DMA((2,)), DMA((2, 4, 2)), DMA((2,)), DMA((3,)), DMA, DMA((2,)),
+            DMA, DMA((2, 2)), DMA, DMA, DMA((2, 4, 2)), DMA, DMA, DMA((2, 4)), DMA, DMA((2, 2)), DMA,
         ],
         compiler_params=pltpu.CompilerParams(collective_id=0, has_side_effects=True, vmem_limit_bytes=63 * 2**20),
         name="layer",
     )(
         query_a, key_a, value_a, query_b, key_b.T, value_b.T, gain_a, gain_b, jnp.asarray(rowtab), jnp.asarray(coltab),
         out_a, out_b, residual.reshape(NX * NC, OWN, D), norm_gain.reshape(1, D), gate_weight, up_weight,
-        down_weight.reshape(2, 3, 128, 128),
+        down_weight.reshape(2, HID, 128),
     )
 
 

time: 114 us -> 106 us (0.930)
  Pallas kernels: 113 us -> 104 us
    pallas_call x1, Pallas kernels: 113 us -> 104 us  [on_device(): pl.pallas_call(layer_kernel, out_shape=jax.ShapeDtypeStruct((OWN, D), BF1...]
where the time goes in v4:
time: 106 us
  Pallas kernels  104 us (98%)
  local copies, waits for them, and re-layouts  1.62 us (2%)
    pallas_call x1, Pallas kernels, on_device(): pl.pallas_call(layer_kernel, out_shape=jax.ShapeDtypeStruct((OWN, D), BF1...  104 us

profile of v4, /device:TPU:1, one launch (start us, length us, event | category | flops | bytes accessed | tf_op | source)
XLA Modules:
  0.0 105.9 jit_solution(11631749371434805912)
XLA Ops:
  0.0 104.3 %layer.1 = bf16[24,4096]{1,0:T(8,128)(2,1)} custom-call(bf16[192,256]{1,0:T(8,128)(2,1)} %qa.1, bf16[192,128]{1,0:T(8,128)(2,1)} %ka.1, bf16[192,128]{1,0:T(8,128)(2,1)} %va.1, bf16[192,256]{1,0:T(8,128)(2,1)} %qb.1, bf16[64,192]{1,0:T(8,128)(2,1)} %bitcast.7, bf16[64,192]{1,0:T(8,128)(2,1)} %bitcast.8, f32[2,128]{1,0:T(2,128)} %gain_a.1, f32[2,64]{1,0:T(2,128)} %gain_b.1, ...), custom_call_target="tpu_custom_call" | custom-call | tf_op jit(solution)/shard_map/layer/pallas_call | solution.py:555
  104.3 1.6 %copy.19 = bf16[24,4096]{1,0:T(8,128)(2,1)} copy(bf16[24,4096]{1,0:T(8,128)(2,1)} %layer.1) | data formatting | bytes 393216

commit v5 on v4

--- a/solution.py
+++ b/solution.py
@@ -58,7 +58,7 @@
     barrier = pltpu.get_barrier_semaphore()
     for device in devices:
         pl.semaphore_signal(barrier, inc=1, device_id=device, device_id_type=MESH)
-    pl.semaphore_wait(barrier, len(devices))
+    return lambda: pl.semaphore_wait(barrier, len(devices))
 
 
 HEADS = 6
@@ -84,6 +84,7 @@
     up_z, down_z = at((z + 1) % NZ, y, x, c), at((z + NZ - 1) % NZ, y, x, c)
     other = at(z, y, x, 1 - c)
 
+    all_greeted = greet(to_y[1:] + [at(z, ys[d], x, 1 - c) for d in range(4)] + to_x[1:] + [up_z, down_z])
     loads = [
         pltpu.make_async_copy(resid.at[x * NC + c], own_resid, l_sem),
         pltpu.make_async_copy(outa_any, outa, o_sem.at[0]),
@@ -132,7 +133,7 @@
         qs[0, t] = turned(qa[:, t * 128 : t * 128 + 128], gain_a[0:1, :], cos_a, sin_a, 128).astype(BF16)
     for t in range(2):
         qs[0, 2 + t] = turned(qb[:, t * 128 : t * 128 + 128], twice(gain_b[0:1, :]), cos_b, sin_b, 64).astype(BF16)
-    greet(to_y[1:] + [at(z, ys[d], x, 1 - c) for d in range(4)] + to_x[1:] + [up_z, down_z])
+    all_greeted()
 
     def kv_step(s, piece):
         copies = []
@@ -157,7 +158,7 @@
     def q_copy(d):
         return send(qs.at[0], qs.at[4 - d], q_send, q_recv.at[d - 1], to_y[d])
 
-    q_copies = {d: q_copy(d) for d in (1, 3, 2)}
+    q_copies = {d: q_copy(d) for d in (1, 3)}
 
     def first_pieces(h):
         return [
@@ -169,17 +170,18 @@
     def stays(h):
         return jnp.logical_and(2 * c + h == y, y // 2 == c)
 
-    for h in range(2):
-
-        @pl.when(stays(h))
-        def _():
-            for src, dst in first_pieces(h):
-                pltpu.make_async_copy(src, dst, wa_local).start()
-
-        @pl.when(jnp.logical_not(stays(h)))
-        def _():
-            for src, dst in first_pieces(h):
-                send(src, dst, wa_send.at[h], wa_recv.at[y % 2], at(z, 2 * c + h, x, y // 2))
+    def first_exchange():
+        for h in range(2):
+
+            @pl.when(stays(h))
+            def _():
+                for src, dst in first_pieces(h):
+                    pltpu.make_async_copy(src, dst, wa_local).start()
+
+            @pl.when(jnp.logical_not(stays(h)))
+            def _():
+                for src, dst in first_pieces(h):
+                    send(src, dst, wa_send.at[h], wa_recv.at[y % 2], at(z, 2 * c + h, x, y // 2))
 
     def w_ref(kind, offset, p):
         return (wgu, wdn)[kind].at[SLOT[offset], 2 * c + p]
@@ -212,6 +214,9 @@
         for p in range(2):
             settle(kv.at[0], kv_recv.at[s - 1, p])
             kv_step(s + 1, p)
+        if s == 1:
+            q_copies[2] = q_copy(2)
+            first_exchange()
 
     contract = (((1,), (1,)), ((), ()))
 
@@ -413,13 +418,13 @@
     w_on(0, 2, 1)
     for h, k in both:
         line[h, k].wait_recv()
-        got = 3 if k == 0 else 1
-        hop(h, k, got, False, 1)
-        for k2 in range(2):
-            plane[h, got, k2] = hop(h, k2, got, True, 0)
+        hop(h, k, 3 if k == 0 else 1, False, 1)
+    for h, k in both:
+        plane[h, 3, k] = hop(h, k, 3, True, 0)
     for h, k in both:
         plane[h, 0, k].wait_recv()
         hop(h, k, 0, True, 1)
+        plane[h, 1, k] = hop(h, k, 1, True, 0)
     w_on(1, 2, 0)
     w_on(1, 2, 1)
     w_on(0, 3, 0)
@@ -485,13 +490,19 @@
     for d2 in order:
         for h, k in both:
             r_move(0, h, d2, k, block(h, 2, d2, k))
-    for d2 in order:
+    def plain(d2):
         for h, k in both:
             r_move(1, h, d2, k, block(h, 1 + 2 * k, d2, 1 - k))
+
+    plain(2)
+    plain(1)
+    for d2 in order:
         settle(r_in.at[0, 0, pl.ds(0, 2)], r_recv.at[0, d2])
         for h, k in both:
             r_add[h, d2, k] = (block(h, 1 + 2 * k, d2, k)[...].astype(F32) + r_in[0, h, d2, k].astype(F32)).astype(BF16)
             r_move(2, h, d2, k, r_add.at[h, d2, k])
+        if d2 in (2, 1):
+            plain({2: 3, 1: 0}[d2])
     totals = {}
 
     def landed(h, d2):

time: 106 us -> 103 us (0.972)
  Pallas kernels: 104 us -> 101 us
    pallas_call x1, Pallas kernels: 104 us -> 101 us  [on_device(): pl.pallas_call(layer_kernel, out_shape=jax.ShapeDtypeStruct((OWN, D), BF1...]
where the time goes in v5:
time: 103 us; the launch traced here: 102 us
  Pallas kernels  101 us (98%)
  local copies, waits for them, and re-layouts  1.62 us (2%)
    pallas_call x1, Pallas kernels, on_device(): pl.pallas_call(layer_kernel, out_shape=jax.ShapeDtypeStruct((OWN, D), BF1...  101 us

profile of v5, /device:TPU:1, one launch (start us, length us, event | category | flops | bytes accessed | tf_op | source)
XLA Modules:
  0.0 102.3 jit_solution(9963538188953311392)
XLA Ops:
  0.0 100.7 %layer.1 = bf16[24,4096]{1,0:T(8,128)(2,1)} custom-call(bf16[192,256]{1,0:T(8,128)(2,1)} %qa.1, bf16[192,128]{1,0:T(8,128)(2,1)} %ka.1, bf16[192,128]{1,0:T(8,128)(2,1)} %va.1, bf16[192,256]{1,0:T(8,128)(2,1)} %qb.1, bf16[64,192]{1,0:T(8,128)(2,1)} %bitcast.7, bf16[64,192]{1,0:T(8,128)(2,1)} %bitcast.8, f32[2,128]{1,0:T(2,128)} %gain_a.1, f32[2,64]{1,0:T(2,128)} %gain_b.1, ...), custom_call_target="tpu_custom_call" | custom-call | tf_op jit(solution)/shard_map/layer/pallas_call | solution.py:566
  100.7 1.6 %copy.19 = bf16[24,4096]{1,0:T(8,128)(2,1)} copy(bf16[24,4096]{1,0:T(8,128)(2,1)} %layer.1) | data formatting | bytes 393216

commit v6 on v5

--- a/solution.py
+++ b/solution.py
@@ -454,7 +454,6 @@
         lined = tokens[:, :, :, cols_of(n)].astype(F32).reshape(count, 512).astype(BF16)
         lhs[:, pl.ds(pl.multiple_of(n * 512, 512), 512)] = lined
 
-    w_on(1, 4, 0)
     settle(wgu.at[:, pl.ds(0, 2)], wc_recv.at[0])
 
     @pl.loop(0, 3)
@@ -462,6 +461,7 @@
         cols = pl.ds(pl.multiple_of(n * 256, 256), 256)
         acc[:, cols] = jnp.dot(lhs[...], wgu[:, :, :, cols].reshape(D, 256), preferred_element_type=F32)
 
+    w_on(1, 4, 0)
     gated = acc[:, 0:HID]
     hidden[...] = (gated / (1.0 + jnp.exp(-gated)) * acc[:, HID : 2 * HID]).astype(BF16)
 

time: 103 us -> 103 us (level)
  no operation moved by 1% of the time
where the time goes in v6:
time: 103 us; the launch traced here: 102 us
  Pallas kernels  101 us (98%)
  local copies, waits for them, and re-layouts  1.62 us (2%)
    pallas_call x1, Pallas kernels, on_device(): pl.pallas_call(layer_kernel, out_shape=jax.ShapeDtypeStruct((OWN, D), BF1...  101 us

profile of v6, /device:TPU:1, one launch (start us, length us, event | category | flops | bytes accessed | tf_op | source)
XLA Modules:
  0.0 102.3 jit_solution(8644667340852811513)
XLA Ops:
  0.0 100.7 %layer.1 = bf16[24,4096]{1,0:T(8,128)(2,1)} custom-call(bf16[192,256]{1,0:T(8,128)(2,1)} %qa.1, bf16[192,128]{1,0:T(8,128)(2,1)} %ka.1, bf16[192,128]{1,0:T(8,128)(2,1)} %va.1, bf16[192,256]{1,0:T(8,128)(2,1)} %qb.1, bf16[64,192]{1,0:T(8,128)(2,1)} %bitcast.7, bf16[64,192]{1,0:T(8,128)(2,1)} %bitcast.8, f32[2,128]{1,0:T(2,128)} %gain_a.1, f32[2,64]{1,0:T(2,128)} %gain_b.1, ...), custom_call_target="tpu_custom_call" | custom-call | tf_op jit(solution)/shard_map/layer/pallas_call | solution.py:566
  100.7 1.6 %copy.19 = bf16[24,4096]{1,0:T(8,128)(2,1)} copy(bf16[24,4096]{1,0:T(8,128)(2,1)} %layer.1) | data formatting | bytes 393216
